TPU v7x, 256 devices: a whole 4x4x8 slice. The times are simulated.
256 devices in a mesh: rep: 2 (over z_hi), fs: 16 (over z_lo, x), tp: 8 (over y, core).
Axes of the slice: x: 4, y: 4, z: 8 (z_hi: 2, z_lo: 4; z = z_hi * 4 + z_lo), core: 2. Of those that a mesh axis runs over, the one named last changes fastest.
Arguments:
- tokens: bfloat16 [32768, 2048], P(('rep', 'fs', 'tp')), may hold values from -6 to 6
- mixer_gain: float32 [2048], replicated, may hold values from 0.1 to 1.9
- direct_weight: float32 [2048, 1024], P('fs', 'tp'), may hold values from -0.125 to 0.125
- direct_scale: float32 [1024], P('tp'), may hold values from 0.5 to 2
- value_weight: float32 [2048, 1024], P('fs', 'tp'), may hold values from -0.125 to 0.125
- value_scale: float32 [1024], P('tp'), may hold values from 0.5 to 8, as said below
- value_gain: float32 [1024], P('tp'), may hold values from 0.1 to 1.9
- value_shift: float32 [1024], P('tp'), may hold values from -3 to 3
- spatial_weight: bfloat16 [16, 128, 128], P('tp'), may hold values from -0.25 to 0.25
- spatial_bias: float32 [16, 128], P('tp'), may hold values from 0.1 to 1.9
- merge_weight: float32 [1024, 2048], P('tp', 'fs'), may hold values from -0.1875 to 0.1875
- merge_scale: float32 [2048], P('fs'), may hold values from 0.5 to 2
- channel_gain: float32 [2048], replicated, may hold values from 0.1 to 1.9
- expand_weight: float32 [2048, 8192], P('fs', 'tp'), may hold values from -0.125 to 0.125
- expand_scale: float32 [8192], P('tp'), may hold values from 0.5 to 2
- reduce_weight: float32 [8192, 2048], P('tp', 'fs'), may hold values from -0.0625 to 0.0625
- reduce_scale: float32 [2048], P('fs'), may hold values from 0.5 to 2
Outputs:
- result: bfloat16 [32768, 2048], P(('rep', 'fs', 'tp'))
Inputs may be any that keep to these rules, and one draw needn't show every extreme that they name: `value_scale`: positive column scales.
All inputs are finite; a program needn't handle non-finite values.
Results may differ from a plain program's by a relative error of at most 0.024.
Values may be sent and summed in bfloat16 or wider, within the bound.
No kernel may reach another device: no remote copies, remote signals or barrier semaphores. Data moves between devices by JAX's collectives and lax.ppermute only.
A program may use at most 64 MiB of HBM per device.

v0:
```python
import jax
import jax.numpy as jnp
from jax import lax
from jax.experimental import pallas as pl
from jax.experimental.pallas import tpu as pltpu
from jax.sharding import Mesh
from jax.sharding import PartitionSpec as P

ALL = ("rep", "z", "x", "y", "core")
FS = ("z", "x")
TP = ("y", "core")
ZRING = ("rep", "z")
EPS = 1e-06
BF = jnp.bfloat16
F32 = jnp.float32
T = 128
HALF = T // 2
D = 2048
AW = 1024
FF_DEV = 1024
K = D // T
PACK = 3 * T + 16
CHUNK = 512


def shift(x, axis, by):
    n = 8 if axis == ZRING else lax.axis_size(axis)
    pairs = [(i, (i + by) % n) for i in range(n)]
    if axis == ZRING and by == 2:
        pairs = [(i, (i + (2 if i % 2 == 0 else -2)) % n) for i in range(n)]
    return lax.ppermute(x, axis, pairs)


def swap(x):
    return lax.ppermute(x, "core", [(0, 1), (1, 0)])


def others(x, axis):
    return (shift(x, axis, -1), shift(x, axis, 2), shift(x, axis, 1))


def gelu(x):
    return 0.5 * x * (1.0 + jnp.tanh(0.7978845608028654 * (x + 0.044715 * x * x * x)))


VM = pl.BlockSpec(memory_space=pltpu.VMEM)
SM = pl.BlockSpec(memory_space=pltpu.SMEM)
HB = pl.BlockSpec(memory_space=pl.ANY)
RAW = pl.BlockSpec(memory_space=pltpu.HBM)


def call(kernel, outs, inputs, specs, scratch, out_specs=None, vmem=8):
    return pl.pallas_call(
        kernel,
        out_shape=[jax.ShapeDtypeStruct(s, d) for s, d in outs],
        in_specs=specs,
        out_specs=out_specs or [VM] * len(outs),
        scratch_shapes=scratch,
        compiler_params=pltpu.CompilerParams(vmem_limit_bytes=vmem * 1024 * 1024),
    )(*inputs)


def rms(floats, gain):
    return floats * lax.rsqrt(jnp.mean(floats * floats, axis=-1, keepdims=True) + EPS) * gain


def rows_of(first, second):
    high = first.astype(BF).astype(F32)
    other = second.astype(BF).astype(F32)
    return [high, first - high, other, second - other]


def copies(pairs, sem):
    started = [pltpu.make_async_copy(src, dst, sem) for src, dst in pairs]
    for c in started:
        c.start()
    return started


def finish(started):
    for c in started:
        c.wait()


def loaded(sources, buffers, sem):
    finish(copies(list(zip(sources, buffers)), sem))


def norm_kernel(*refs):
    sources, out, buffers, sem = refs[:6], refs[6], refs[7:13], refs[13]
    loaded(sources, buffers, sem)
    tokens, gain, spatial, value_gain, value_shift, bias = buffers
    normed = rms(tokens[...].astype(F32), gain[...]).astype(BF)
    for k in range(K):
        out[k * T : (k + 1) * T] = normed[:, k * T : (k + 1) * T]
    out[D : D + 2 * T] = spatial[...]
    tall = jnp.concatenate([*rows_of(bias[0:1], bias[1:2]), jnp.zeros((T - 4, T), F32)], axis=0)
    out[D + 2 * T : D + 3 * T] = tall.T.astype(BF)
    gains = [*rows_of(value_gain[...], value_shift[...]), jnp.zeros((12, T), F32)]
    out[D + 3 * T : D + PACK] = jnp.concatenate(gains, axis=0).astype(BF)


def columns_kernel(*refs):
    sources, out, buffers, sem = refs[:6], refs[6], refs[7:13], refs[13]
    loaded(sources, buffers, sem)
    at = 0
    for weight, scale in zip(buffers[0::2], buffers[1::2]):
        width = weight.shape[1]
        out[:, at : at + width] = (weight[...] * scale[...]).astype(BF)
        at += width


def merge_kernel(*refs):
    sources, out, buffers, sem = refs[:2], refs[2], refs[3:5], refs[5]
    loaded(sources, buffers, sem)
    out[...] = (buffers[0][...] * buffers[1][...]).astype(BF)


def rows_kernel(m0, m1, m2, m3, weight, scale, out, weight_buffer, scale_buffer, sem):
    started = copies([(weight, weight_buffer), (scale, scale_buffer)], sem)
    for r, part in enumerate((m0, m1, m2, m3)):
        out[r * T : (r + 1) * T] = part[...]
    finish(started)
    out[4 * T :] = (weight_buffer[...] * scale_buffer[...]).astype(BF)


def split_columns_kernel(c0, c1, c2, c3, first, second):
    for n, part in enumerate((c0, c1, c2, c3)):
        first[n] = part[:, : first.shape[2]]
        second[n] = part[:, first.shape[2] :]


def split_rows_kernel(r0, r1, r2, r3, first, second):
    for n, part in enumerate((r0, r1, r2, r3)):
        first[n] = part[: first.shape[1]]
        second[n] = part[first.shape[1] :]


def plus_kernel(near, back, low, high, near_out, back_out):
    near_out[:HALF] = (near[:HALF].astype(F32) + low[...].astype(F32)).astype(BF)
    near_out[HALF:] = near[HALF:]
    back_out[:HALF] = back[:HALF]
    back_out[HALF:] = (back[HALF:].astype(F32) + high[...].astype(F32)).astype(BF)


def prepared(kernel, out, raw, ready=()):
    buffers = [pltpu.VMEM(a.shape, a.dtype) for a in raw]
    return call(
        kernel,
        [(out, BF)],
        (*ready, *[pltpu.with_memory_space_constraint(a, pltpu.HBM) for a in raw]),
        [VM] * len(ready) + [RAW] * len(raw),
        [*buffers, pltpu.SemaphoreType.DMA(())],
    )[0]


def place_of(idx, zr, xr):
    return lax.rem(idx[0] + zr, 4) * 4 + lax.rem(idx[1] + xr, 4)


def aligned(x):
    return pl.multiple_of(x * T, T)


def join_kernel(*refs):
    sources, out, sem = refs[:-2], refs[-2], refs[-1]
    pairs, at = [], 0
    for source in sources:
        pairs.append((source, out.at[at : at + source.shape[0]]))
        at += source.shape[0]
    finish(copies(pairs, sem))


def halves_kernel(near, back, low, high, sem):
    finish(copies([(back.at[:2], low), (near.at[2:], high)], sem))


def joined(arrays):
    shape = (sum(a.shape[0] for a in arrays), *arrays[0].shape[1:])
    sem = [pltpu.SemaphoreType.DMA(())]
    return call(join_kernel, [(shape, BF)], arrays, [HB] * len(arrays), sem)[0]


def dv_kernel(idx, *refs):
    weights = refs[:2]
    sources = refs[2:6]
    out, pack, weight, rows, sem = refs[6:]
    pairs = []
    for q in range(2):
        for zr in range(4):
            for xr in range(4):
                row = aligned(place_of(idx, zr, xr))
                dst = weight.at[pl.ds(row, T), 2 * q * T : 2 * (q + 1) * T]
                pairs.append((weights[q].at[4 * zr + xr], dst))
    for g, source in enumerate(sources):
        pairs.append((source.at[D : D + PACK], pack.at[g]))
    started = copies(pairs, sem)

    def block(source, g, k):
        at = pl.multiple_of(k * T, T)
        return pltpu.make_async_copy(source.at[pl.ds(at, T)], rows.at[g, :, pl.ds(at, T)], sem)

    for g, source in enumerate(sources):
        pl.loop(0, K)(lambda k: block(source, g, k).start())
    finish(started)
    for g, source in enumerate(sources):
        pl.loop(0, K)(lambda k: block(source, g, k).wait())

    @pl.loop(0, 4)
    def _(g):
        part = jnp.dot(rows[g], weight[...], preferred_element_type=F32)
        out[lax.rem(idx[2] + g, 4)] = gelu(part).astype(BF)


def mixer_kernel(idx, tokens, gain, parts, pack_own, pack_partner, *rest):
    merges = rest[:2]
    middle, normed, weight, gated, sem = rest[2:]
    pairs = []
    for q in range(2):
        for zr in range(4):
            for xr in range(4):
                col = aligned(place_of(idx, zr, xr))
                dst = weight.at[4 * q * T : 4 * (q + 1) * T, pl.ds(col, T)]
                pairs.append((merges[q].at[4 * xr + zr], dst))
    started = copies(pairs, sem)

    def moments(y, sums):
        value = [parts[y, :, (2 * q + 1) * T : (2 * q + 2) * T].astype(F32) for q in range(2)]
        total = jnp.sum(value[0] + value[1], axis=1, keepdims=True)
        squares = jnp.sum(value[0] * value[0] + value[1] * value[1], axis=1, keepdims=True)
        return sums[0] + total, sums[1] + squares

    nothing = jnp.zeros((T, 1), F32)
    total, squares = lax.fori_loop(0, 4, moments, (nothing, nothing))
    mean = total * (1.0 / AW)
    var = squares * (1.0 / AW) - mean * mean
    scale = lax.rsqrt(var + EPS)
    lane = lax.broadcasted_iota(jnp.int32, (T, T), 1)

    @pl.loop(0, 4)
    def _(r):
        y = lax.rem(idx[2] + r, 4)
        for q, pack in enumerate((pack_own, pack_partner)):
            gains = pack[r, 3 * T : 3 * T + 16].astype(F32)
            gain_row = gains[0:1] + gains[1:2]
            shift_row = gains[2:3] + gains[3:4]
            bias = pack[r, 2 * T : 3 * T].astype(F32)
            bias_low = bias[:, 0:1] + bias[:, 1:2]
            bias_high = bias[:, 2:3] + bias[:, 3:4]
            value = parts[y, :, (2 * q + 1) * T : (2 * q + 2) * T].astype(F32)
            ready = ((value - mean) * scale * gain_row + shift_row).astype(BF)
            left = jnp.dot(pack[r, 0:T], ready, preferred_element_type=F32) + bias_low
            right = jnp.dot(pack[r, T : 2 * T], ready, preferred_element_type=F32) + bias_high
            mixed = jnp.where(lane < T // 2, left, right)
            direct = parts[y, :, 2 * q * T : (2 * q + 1) * T].astype(F32)
            gated[:, pl.ds(pl.multiple_of((4 * q + r) * T, T), T)] = (direct * mixed).astype(BF)

    finish(started)

    @pl.loop(0, D // CHUNK)
    def _(n):
        cols = pl.ds(pl.multiple_of(n * CHUNK, CHUNK), CHUNK)
        mix = jnp.dot(gated[...], weight[:, cols], preferred_element_type=F32)
        middle[:, cols] = (tokens[:, cols].astype(F32) + mix).astype(BF)

    normed[...] = rms(middle[...].astype(F32), gain[...]).astype(BF)


def picked(parts, n, k):
    near, far = parts
    return far.at[k] if n == 2 else near.at[(0, 4, None, 8)[n] + k]


def up_kernel(idx, *refs):
    out, sem = refs[4:]
    pairs = []
    for q in range(2):
        for zr in range(4):
            for xr in range(4):
                at = aligned(place_of(idx, zr, xr))
                dst = out.at[pl.ds(at, T), q * FF_DEV : (q + 1) * FF_DEV]
                pairs.append((picked(refs[2 * q : 2 * q + 2], zr, xr), dst))
    finish(copies(pairs, sem))


def down_kernel(idx, *refs):
    out, sem = refs[4:]
    pairs = []
    for q in range(2):
        for zr in range(4):
            for xr in range(4):
                at = aligned(place_of(idx, zr, xr))
                dst = out.at[q * FF_DEV : (q + 1) * FF_DEV, pl.ds(at, T)]
                pairs.append((picked(refs[2 * q : 2 * q + 2], xr, zr), dst))
    finish(copies(pairs, sem))


def ff_kernel(groups, up, down, *refs):
    tokens = refs[:groups]
    outs = refs[groups:-2]
    rows, hidden = refs[-2:]
    for g, t in enumerate(tokens):
        rows[g * T : (g + 1) * T] = t[...]

    @pl.loop(0, D // CHUNK)
    def _(n):
        cols = pl.ds(pl.multiple_of(n * CHUNK, CHUNK), CHUNK)
        pre = jnp.dot(rows[...], up[:, cols], preferred_element_type=F32)
        hidden[:, cols] = jnp.square(jnp.maximum(pre, 0.0)).astype(BF)

    @pl.loop(0, D // CHUNK)
    def _(n):
        cols = pl.ds(pl.multiple_of(n * CHUNK, CHUNK), CHUNK)
        part = jnp.dot(hidden[...], down[:, cols], preferred_element_type=F32).astype(BF)
        height = outs[0].shape[0]
        for g, out in enumerate(outs):
            out[:, cols] = part[g * height : (g + 1) * height]


def ff(up, down, tokens, height=T):
    groups = len(tokens)
    return call(
        lambda *refs: ff_kernel(groups, *refs),
        [((height, D), BF)] * (groups * T // height),
        (up, down, *tokens),
        [VM] * (2 + groups),
        [pltpu.VMEM((groups * T, D), BF), pltpu.VMEM((groups * T, D), BF)],
    )


def around(stack, second):
    near = shift(stack, second, -1)
    back = shift(stack, second, 1)
    low, high = call(
        halves_kernel,
        [((2, *stack.shape[1:]), BF)] * 2,
        (near, back),
        [HB] * 2,
        [pltpu.SemaphoreType.DMA(())],
    )
    far_low = shift(low, second, 1)
    far_high = shift(high, second, -1)
    mine = (joined((stack, near, back)), joined((far_low, far_high)))
    return (*mine, *[swap(m) for m in mine])


def layer(
    tokens,
    mixer_gain,
    direct_weight,
    direct_scale,
    value_weight,
    value_scale,
    value_gain,
    value_shift,
    spatial_weight,
    spatial_bias,
    merge_weight,
    merge_scale,
    channel_gain,
    expand_weight,
    expand_scale,
    reduce_weight,
    reduce_scale,
):
    idx = jnp.stack([lax.axis_index(a) for a in ("z", "x", "y")]).astype(jnp.int32)
    row = lambda v: v.reshape(1, -1)
    merge_half = prepared(merge_kernel, (T, T), (merge_weight, row(merge_scale)))
    merge_y = others(merge_half, "y")
    columns = prepared(
        columns_kernel,
        (T, 2 * T + FF_DEV),
        (
            direct_weight,
            row(direct_scale),
            value_weight,
            row(value_scale),
            expand_weight,
            row(expand_scale),
        ),
    )
    columns_x = (columns, *others(columns, "x"))
    normed = prepared(
        norm_kernel,
        (D + PACK, T),
        (
            tokens,
            row(mixer_gain),
            spatial_weight.reshape(2 * T, T),
            row(value_gain),
            row(value_shift),
            spatial_bias,
        ),
    )
    near_rows, far_rows, back_rows = others(normed, "y")
    rows = prepared(
        rows_kernel, (4 * T + FF_DEV, T), (reduce_weight, row(reduce_scale)), (merge_half, *merge_y)
    )
    rows_z = (rows, *others(rows, ZRING))
    dv_stack, expand_stack = call(
        split_columns_kernel, [((4, T, 2 * T), BF), ((4, T, FF_DEV), BF)], columns_x, [VM] * 4, []
    )
    dv_own = joined((dv_stack, *others(dv_stack, ZRING)))
    dv_partner = swap(dv_own)
    merge_stack, reduce_stack = call(
        split_rows_kernel, [((4, 4 * T, T), BF), ((4, FF_DEV, T), BF)], rows_z, [VM] * 4, []
    )
    merge_own = joined((merge_stack, *others(merge_stack, "x")))
    merge_partner = swap(merge_own)
    expands = around(expand_stack, ZRING)
    reduces = around(reduce_stack, "x")

    parts, pack_own = call(
        dv_kernel,
        [((4, T, 4 * T), BF), ((4, PACK, T), BF)],
        (idx, dv_own, dv_partner, normed, near_rows, far_rows, back_rows),
        [SM] + [HB] * 6,
        [
            pltpu.VMEM((D, 4 * T), BF),
            pltpu.VMEM((4, T, D), BF),
            pltpu.SemaphoreType.DMA(()),
        ],
        [VM, HB],
        16,
    )
    parts = lax.all_to_all(parts, "y", 0, 0, tiled=True)
    pack_partner = swap(pack_own)

    middle, normed = call(
        mixer_kernel,
        [((T, D), BF), ((T, D), BF)],
        (
            idx,
            tokens,
            channel_gain.reshape(1, D),
            parts,
            pack_own,
            pack_partner,
            merge_own,
            merge_partner,
        ),
        [SM] + [VM] * 5 + [HB] * 2,
        [pltpu.VMEM((AW, D), BF), pltpu.VMEM((T, AW), BF), pltpu.SemaphoreType.DMA(())],
        None,
        16,
    )
    near_rows, far_rows, back_rows = others(normed, "y")
    dma = [pltpu.SemaphoreType.DMA(())]
    (up,) = call(up_kernel, [((D, 2 * FF_DEV), BF)], (idx, *expands), [SM] + [HB] * 4, dma)
    (down,) = call(down_kernel, [((2 * FF_DEV, D), BF)], (idx, *reduces), [SM] + [HB] * 4, dma)
    far_low, far_high = ff(up, down, (far_rows,), HALF)
    near, back = ff(up, down, (near_rows, back_rows))
    (own,) = ff(up, down, (normed,))
    relay_low = shift(far_low, "y", 1)
    relay_high = shift(far_high, "y", -1)
    near, back = call(
        plus_kernel, [((T, D), BF)] * 2, (near, back, relay_low, relay_high), [VM] * 4, []
    )
    got_back = shift(near, "y", 1)
    got_near = shift(back, "y", -1)
    lower = own.astype(F32) + (got_back.astype(F32) + got_near.astype(F32))
    return (middle.astype(F32) + lower).astype(BF)


def solution(mesh):
    finer = Mesh(mesh.devices.reshape(2, 4, 4, 4, 2), ALL)
    in_specs = (
        P(ALL, None),
        P(),
        P(FS, TP),
        P(TP),
        P(FS, TP),
        P(TP),
        P(TP),
        P(TP),
        P(TP, None, None),
        P(TP, None),
        P(TP, FS),
        P(FS),
        P(),
        P(FS, TP),
        P(TP),
        P(TP, FS),
        P(FS),
    )
    return jax.shard_map(layer, mesh=finer, in_specs=in_specs, out_specs=P(ALL, None), check_vma=False)
```

profile of v0, /device:TPU:2, one launch (start us, length us, event | category | flops | bytes accessed | tf_op | source)
XLA Modules:
  0.0 220.0 jit_solution(1691249972613727516)
XLA Ops:
  5.1 3.1 %collective-permute-start.11 = (bf16[128,128]{1,0:T(8,128)(2,1)S(1)}, bf16[128,128]{1,0:T(8,128)(2,1)S(1)}, u32[]{:S(2)}, u32[]{:S(2)}) collective-permute-start(bf16[128,128]{1,0:T(8,128)(2,1)S(1)} %shard_map.168.m0), channel_id=1, source_target_pairs={{0,6},{2,0},{4,2},{6,4},{1,7},{3,1},{5,3},{7,5},{8,14},{10,8},{12,... | collective-permute-start | bytes 98312 | tf_op jit(solution)/shard_map/ppermute | solution.py:31
  9.8 3.8 %collective-permute-done.12.m2 = bf16[128,128]{1,0:T(8,128)(2,1)S(1)} collective-permute-done((bf16[128,128]{1,0:T(8,128)(2,1)S(1)}, bf16[128,128]{1,0:T(8,128)(2,1)S(1)}, u32[]{:S(2)}, u32[]{:S(2)}) %collective-permute-start.12) | collective-permute-done | bytes 32800 | tf_op jit(solution)/shard_map/ppermute | solution.py:31
  15.0 5.9 %collective-permute-start.14 = (bf16[1536,128]{1,0:T(8,128)(2,1)S(1)}, bf16[1536,128]{1,0:T(8,128)(2,1)S(1)}, u32[]{:S(2)}, u32[]{:S(2)}) collective-permute-start(bf16[1536,128]{1,0:T(8,128)(2,1)S(1)} %shard_map.169.r0), channel_id=1, source_target_pairs={{0,224},{32,0},{64,32},{96,64},{128,96},{160,128},{192,160},{224,1... | collective-permute-start | bytes 1179656 | tf_op jit(solution)/shard_map/ppermute | solution.py:31
  30.7 10.1 %collective-permute-done.14.r1 = bf16[1536,128]{1,0:T(8,128)(2,1)S(1)} collective-permute-done((bf16[1536,128]{1,0:T(8,128)(2,1)S(1)}, bf16[1536,128]{1,0:T(8,128)(2,1)S(1)}, u32[]{:S(2)}, u32[]{:S(2)}) %collective-permute-start.14) | collective-permute-done | bytes 393248 | tf_op jit(solution)/shard_map/ppermute | solution.py:31
  40.8 3.8 %collective-permute-start.21 = (bf16[4,128,1024]{2,1,0:T(8,128)(2,1)S(1)}, bf16[4,128,1024]{2,1,0:T(8,128)(2,1)S(1)}, u32[]{:S(2)}, u32[]{:S(2)}) collective-permute-start(bf16[4,128,1024]{2,1,0:T(8,128)(2,1)S(1)} %get-tuple-element.28.refs_0_), channel_id=1, source_target_pairs={{0,224},{32,0},{64,32},{96,64},{128,96},{160,128},{192,160},{224,1... | collective-permute-start | bytes 3145736 | tf_op jit(solution)/shard_map/ppermute | solution.py:31
  48.3 3.6 %collective-permute-done.4.refs_2_ = bf16[4,128,256]{2,1,0:T(8,128)(2,1)S(1)} collective-permute-done((bf16[4,128,256]{2,1,0:T(8,128)(2,1)S(1)}, bf16[4,128,256]{2,1,0:T(8,128)(2,1)S(1)}, u32[]{:S(2)}, u32[]{:S(2)}) %collective-permute-start.4) | collective-permute-done | bytes 262176 | tf_op jit(solution)/shard_map/ppermute | solution.py:31
  51.8 4.4 %collective-permute-done.5.refs_3_ = bf16[4,128,256]{2,1,0:T(8,128)(2,1)S(1)} collective-permute-done((bf16[4,128,256]{2,1,0:T(8,128)(2,1)S(1)}, bf16[4,128,256]{2,1,0:T(8,128)(2,1)S(1)}, u32[]{:S(2)}, u32[]{:S(2)}) %collective-permute-start.5) | collective-permute-done | bytes 262176 | tf_op jit(solution)/shard_map/ppermute | solution.py:31
  58.3 24.4 %collective-permute-done.17.refs_1_ = bf16[4,512,128]{2,1,0:T(8,128)(2,1)S(1)} collective-permute-done((bf16[4,512,128]{2,1,0:T(8,128)(2,1)S(1)}, bf16[4,512,128]{2,1,0:T(8,128)(2,1)S(1)}, u32[]{:S(2)}, u32[]{:S(2)}) %collective-permute-start.17) | collective-permute-done | bytes 524320 | tf_op jit(solution)/shard_map/ppermute | solution.py:31
  82.7 5.2 %collective-permute-start.18 = (bf16[4,512,128]{2,1,0:T(8,128)(2,1)S(1)}, bf16[4,512,128]{2,1,0:T(8,128)(2,1)S(1)}, u32[]{:S(2)}, u32[]{:S(2)}) collective-permute-start(bf16[4,512,128]{2,1,0:T(8,128)(2,1)S(1)} %get-tuple-element.26.refs_0_), channel_id=1, source_target_pairs={{0,16},{8,24},{16,0},{24,8},{1,17},{9,25},{17,1},{25,9},{2,18},{10... | collective-permute-start | bytes 1572872 | tf_op jit(solution)/shard_map/ppermute | solution.py:31
  92.1 2.9 %collective-permute-done.18.refs_2_ = bf16[4,512,128]{2,1,0:T(8,128)(2,1)S(1)} collective-permute-done((bf16[4,512,128]{2,1,0:T(8,128)(2,1)S(1)}, bf16[4,512,128]{2,1,0:T(8,128)(2,1)S(1)}, u32[]{:S(2)}, u32[]{:S(2)}) %collective-permute-start.18) | collective-permute-done | bytes 524320 | tf_op jit(solution)/shard_map/ppermute | solution.py:31
  95.0 6.6 %collective-permute-done.19.refs_3_ = bf16[4,512,128]{2,1,0:T(8,128)(2,1)S(1)} collective-permute-done((bf16[4,512,128]{2,1,0:T(8,128)(2,1)S(1)}, bf16[4,512,128]{2,1,0:T(8,128)(2,1)S(1)}, u32[]{:S(2)}, u32[]{:S(2)}) %collective-permute-start.19) | collective-permute-done | bytes 524320 | tf_op jit(solution)/shard_map/ppermute | solution.py:31
  103.0 4.4 %collective-permute-done.8.refs_4_ = bf16[2448,128]{1,0:T(8,128)(2,1)S(1)} collective-permute-done((bf16[2448,128]{1,0:T(8,128)(2,1)S(1)}, bf16[2448,128]{1,0:T(8,128)(2,1)S(1)}, u32[]{:S(2)}, u32[]{:S(2)}) %collective-permute-start.8) | collective-permute-done | bytes 626720 | tf_op jit(solution)/shard_map/ppermute | solution.py:31
  107.5 12.4 %collective-permute-done.9.refs_5_ = bf16[2448,128]{1,0:T(8,128)(2,1)S(1)} collective-permute-done((bf16[2448,128]{1,0:T(8,128)(2,1)S(1)}, bf16[2448,128]{1,0:T(8,128)(2,1)S(1)}, u32[]{:S(2)}, u32[]{:S(2)}) %collective-permute-start.9) | collective-permute-done | bytes 626720 | tf_op jit(solution)/shard_map/ppermute | solution.py:31
  124.3 10.6 %collective-permute-done.23.refs_0_ = bf16[2,128,1024]{2,1,0:T(8,128)(2,1)S(1)} collective-permute-done((bf16[2,128,1024]{2,1,0:T(8,128)(2,1)S(1)}, bf16[2,128,1024]{2,1,0:T(8,128)(2,1)S(1)}, u32[]{:S(2)}, u32[]{:S(2)}) %collective-permute-start.23) | collective-permute-done | bytes 524320 | tf_op jit(solution)/shard_map/ppermute | solution.py:31
  146.6 4.9 %shard_map.167 = (bf16[4,128,512]{2,1,0:T(8,128)(2,1)S(1)}, bf16[4,400,128]{2,1,0:T(8,128)(2,1)S(1)}) custom-call(s32[3]{0:T(128)S(1)} %pad_add_fusion.idx, bf16[16,128,256]{2,1,0:T(8,128)(2,1)S(1)} %copy-done.1, bf16[16,128,256]{2,1,0:T(8,128)(2,1)S(1)} %copy-done.6, bf16[2448,128]{1,0:T(8,128)(2,1)S(1)} %copy-done.3, bf16[2448,128]{1,0:T(8,128)(2,1)S(1)} %copy-done.8, ...), custom_call_target="tpu_custom_call" | custom-call | tf_op jit(solution)/shard_map/pallas_call | solution.py:53
  154.1 12.6 %all_to_all.5.parts = bf16[4,128,512]{2,1,0:T(8,128)(2,1)S(1)} all-to-all(bf16[4,128,512]{2,1,0:T(8,128)(2,1)S(1)} %get-tuple-element.24), channel_id=1, replica_groups=mesh['rep'=2,'z'=4,'x'=4,'y'=4,'core'=2] {'y'}, dimensions={0} | all-to-all | bytes 1048576 | tf_op jit(solution)/shard_map/all_to_all | solution.py:426
  166.7 4.3 %shard_map.172 = (bf16[128,2048]{1,0:T(8,128)(2,1)S(1)}, bf16[128,2048]{1,0:T(8,128)(2,1)S(1)}) custom-call(s32[3]{0:T(128)S(1)} %pad_add_fusion.idx, bf16[128,2048]{1,0:T(8,128)(2,1)S(1)} %copy-done.4, f32[1,2048]{1,0:T(1,128)S(1)} %bitcast.13, bf16[4,128,512]{2,1,0:T(8,128)(2,1)S(1)} %all_to_all.5.parts, ...), custom_call_target="tpu_custom_call" | custom-call | tf_op jit(solution)/shard_map/pallas_call | solution.py:53
  174.3 2.7 %shard_map.176.refs_0_ = bf16[2048,2048]{1,0:T(8,128)(2,1)S(1)} custom-call(s32[3]{0:T(128)S(1)} %pad_add_fusion.idx, bf16[12,128,1024]{2,1,0:T(8,128)(2,1)S(1)} %shard_map.173.refs_0_, bf16[4,128,1024]{2,1,0:T(8,128)(2,1)S(1)} %shard_map.175.refs_1_, bf16[12,128,1024]{2,1,0:T(8,128)(2,1)} %collective-permute-done.25.refs_2_, ...), custom_call_target="tpu_custom_call" | custom-call | tf_op jit(solution)/shard_map/pallas_call | solution.py:53
  177.1 3.5 %shard_map.180.refs_1_ = bf16[2048,2048]{1,0:T(8,128)(2,1)S(1)} custom-call(s32[3]{0:T(128)S(1)} %pad_add_fusion.idx, bf16[12,1024,128]{2,1,0:T(8,128)(2,1)} %shard_map.177.refs_0_, bf16[4,1024,128]{2,1,0:T(8,128)(2,1)S(1)} %shard_map.179.refs_1_, bf16[12,1024,128]{2,1,0:T(8,128)(2,1)} %collective-permute-done.31.refs_2_, ...), custom_call_target="tpu_custom_call" | custom-call | tf_op jit(solution)/shard_map/pallas_call | solution.py:53
  180.6 6.8 %collective-permute-done.35.refs_2_ = bf16[128,2048]{1,0:T(8,128)(2,1)S(1)} collective-permute-done((bf16[128,2048]{1,0:T(8,128)(2,1)S(1)}, bf16[128,2048]{1,0:T(8,128)(2,1)S(1)}, u32[]{:S(2)}, u32[]{:S(2)}) %collective-permute-start.35) | collective-permute-done | bytes 524320 | tf_op jit(solution)/shard_map/ppermute | solution.py:31
  187.4 3.7 %shard_map.183 = (bf16[64,2048]{1,0:T(8,128)(2,1)S(1)}, bf16[64,2048]{1,0:T(8,128)(2,1)S(1)}) custom-call(bf16[2048,2048]{1,0:T(8,128)(2,1)S(1)} %shard_map.176.refs_0_, bf16[2048,2048]{1,0:T(8,128)(2,1)S(1)} %shard_map.180.refs_1_, bf16[128,2048]{1,0:T(8,128)(2,1)S(1)} %collective-permute-done.35.refs_2_), custom_call_target="tpu_custom_call" | custom-call | tf_op jit(solution)/shard_map/pallas_call | solution.py:53
  197.2 5.8 %shard_map.182 = (bf16[128,2048]{1,0:T(8,128)(2,1)S(1)}, bf16[128,2048]{1,0:T(8,128)(2,1)S(1)}) custom-call(bf16[2048,2048]{1,0:T(8,128)(2,1)S(1)} %shard_map.176.refs_0_, bf16[2048,2048]{1,0:T(8,128)(2,1)S(1)} %shard_map.180.refs_1_, bf16[128,2048]{1,0:T(8,128)(2,1)S(1)} %collective-permute-done.33.refs_2_, ...), custom_call_target="tpu_custom_call" | custom-call | tf_op jit(solution)/shard_map/pallas_call | solution.py:53
  205.3 3.7 %shard_map.181 = bf16[128,2048]{1,0:T(8,128)(2,1)S(1)} custom-call(bf16[2048,2048]{1,0:T(8,128)(2,1)S(1)} %shard_map.176.refs_0_, bf16[2048,2048]{1,0:T(8,128)(2,1)S(1)} %shard_map.180.refs_1_, bf16[128,2048]{1,0:T(8,128)(2,1)S(1)} %get-tuple-element.34.refs_2_), custom_call_target="tpu_custom_call" | custom-call | tf_op jit(solution)/shard_map/pallas_call | solution.py:53
  209.0 7.8 %collective-permute-done.39 = bf16[128,2048]{1,0:T(8,128)(2,1)S(1)} collective-permute-done((bf16[128,2048]{1,0:T(8,128)(2,1)S(1)}, bf16[128,2048]{1,0:T(8,128)(2,1)S(1)}, u32[]{:S(2)}, u32[]{:S(2)}) %collective-permute-start.39) | collective-permute-done | bytes 524320 | tf_op jit(solution)/shard_map/ppermute | solution.py:31
  (117 shorter events, 62.6 us)
Async XLA Ops:
  1.2 21.6 %collective-permute-start = (bf16[128,1280]{1,0:T(8,128)(2,1)S(1)}, bf16[128,1280]{1,0:T(8,128)(2,1)S(1)}, u32[]{:S(2)}, u32[]{:S(2)}) collective-permute-start(bf16[128,1280]{1,0:T(8,128)(2,1)S(1)} %shard_map.163.c0), channel_id=1, source_target_pairs={{0,24},{8,0},{16,8},{24,16},{1,25},{9,1},{17,9},{25,17},{2,26},{10... | collective-permute-start | bytes 983048 | tf_op jit(solution)/shard_map/ppermute | solution.py:31
  3.5 23.1 %collective-permute-start.1 = (bf16[128,1280]{1,0:T(8,128)(2,1)S(1)}, bf16[128,1280]{1,0:T(8,128)(2,1)S(1)}, u32[]{:S(2)}, u32[]{:S(2)}) collective-permute-start(bf16[128,1280]{1,0:T(8,128)(2,1)S(1)} %shard_map.163.c0), channel_id=1, source_target_pairs={{0,16},{8,24},{16,0},{24,8},{1,17},{9,25},{17,1},{25,9},{2,18},{10... | collective-permute-start | bytes 983048 | tf_op jit(solution)/shard_map/ppermute | solution.py:31
  15.0 25.8 %collective-permute-start.14 = (bf16[1536,128]{1,0:T(8,128)(2,1)S(1)}, bf16[1536,128]{1,0:T(8,128)(2,1)S(1)}, u32[]{:S(2)}, u32[]{:S(2)}) collective-permute-start(bf16[1536,128]{1,0:T(8,128)(2,1)S(1)} %shard_map.169.r0), channel_id=1, source_target_pairs={{0,224},{32,0},{64,32},{96,64},{128,96},{160,128},{192,160},{224,1... | collective-permute-start | bytes 1179656 | tf_op jit(solution)/shard_map/ppermute | solution.py:31
  21.0 19.9 %collective-permute-start.15 = (bf16[1536,128]{1,0:T(8,128)(2,1)S(1)}, bf16[1536,128]{1,0:T(8,128)(2,1)S(1)}, u32[]{:S(2)}, u32[]{:S(2)}) collective-permute-start(bf16[1536,128]{1,0:T(8,128)(2,1)S(1)} %shard_map.169.r0), channel_id=1, source_target_pairs={{0,64},{32,224},{64,128},{96,32},{128,192},{160,96},{192,0},{224,1... | collective-permute-start | bytes 1179656 | tf_op jit(solution)/shard_map/ppermute | solution.py:31
  22.8 21.9 %collective-permute-start.16 = (bf16[1536,128]{1,0:T(8,128)(2,1)S(1)}, bf16[1536,128]{1,0:T(8,128)(2,1)S(1)}, u32[]{:S(2)}, u32[]{:S(2)}) collective-permute-start(bf16[1536,128]{1,0:T(8,128)(2,1)S(1)} %shard_map.169.r0), channel_id=1, source_target_pairs={{0,32},{32,64},{64,96},{96,128},{128,160},{160,192},{192,224},{224... | collective-permute-start | bytes 1179656 | tf_op jit(solution)/shard_map/ppermute | solution.py:31
  26.6 31.4 %collective-permute-start.7 = (bf16[2448,128]{1,0:T(8,128)(2,1)S(1)}, bf16[2448,128]{1,0:T(8,128)(2,1)S(1)}, u32[]{:S(2)}, u32[]{:S(2)}) collective-permute-start(bf16[2448,128]{1,0:T(8,128)(2,1)S(1)} %shard_map.166.refs_2_), channel_id=1, source_target_pairs={{0,6},{2,0},{4,2},{6,4},{1,7},{3,1},{5,3},{7,5},{8,14},{10,8},{12,... | collective-permute-start | bytes 1880072 | tf_op jit(solution)/shard_map/ppermute | solution.py:31
  28.3 18.3 %collective-permute-start.3 = (bf16[4,128,256]{2,1,0:T(8,128)(2,1)S(1)}, bf16[4,128,256]{2,1,0:T(8,128)(2,1)S(1)}, u32[]{:S(2)}, u32[]{:S(2)}) collective-permute-start(bf16[4,128,256]{2,1,0:T(8,128)(2,1)S(1)} %get-tuple-element.23.refs_0_), channel_id=1, source_target_pairs={{0,224},{32,0},{64,32},{96,64},{128,96},{160,128},{192,160},{224,1... | collective-permute-start | bytes 786440 | tf_op jit(solution)/shard_map/ppermute | solution.py:31
  40.8 47.0 %collective-permute-start.21 = (bf16[4,128,1024]{2,1,0:T(8,128)(2,1)S(1)}, bf16[4,128,1024]{2,1,0:T(8,128)(2,1)S(1)}, u32[]{:S(2)}, u32[]{:S(2)}) collective-permute-start(bf16[4,128,1024]{2,1,0:T(8,128)(2,1)S(1)} %get-tuple-element.28.refs_0_), channel_id=1, source_target_pairs={{0,224},{32,0},{64,32},{96,64},{128,96},{160,128},{192,160},{224,1... | collective-permute-start | bytes 3145736 | tf_op jit(solution)/shard_map/ppermute | solution.py:31
  46.6 41.3 %collective-permute-start.22 = (bf16[4,128,1024]{2,1,0:T(8,128)(2,1)S(1)}, bf16[4,128,1024]{2,1,0:T(8,128)(2,1)S(1)}, u32[]{:S(2)}, u32[]{:S(2)}) collective-permute-start(bf16[4,128,1024]{2,1,0:T(8,128)(2,1)S(1)} %get-tuple-element.28.refs_0_), channel_id=1, source_target_pairs={{0,32},{32,64},{64,96},{96,128},{128,160},{160,192},{192,224},{224... | collective-permute-start | bytes 3145736 | tf_op jit(solution)/shard_map/ppermute | solution.py:31
  51.8 36.4 %collective-permute-start.27 = (bf16[4,1024,128]{2,1,0:T(8,128)(2,1)S(1)}, bf16[4,1024,128]{2,1,0:T(8,128)(2,1)S(1)}, u32[]{:S(2)}, u32[]{:S(2)}) collective-permute-start(bf16[4,1024,128]{2,1,0:T(8,128)(2,1)S(1)} %get-tuple-element.31.refs_0_), channel_id=1, source_target_pairs={{0,24},{8,0},{16,8},{24,16},{1,25},{9,1},{17,9},{25,17},{2,26},{10... | collective-permute-start | bytes 3145736 | tf_op jit(solution)/shard_map/ppermute | solution.py:31
  56.3 32.6 %collective-permute-start.28 = (bf16[4,1024,128]{2,1,0:T(8,128)(2,1)S(1)}, bf16[4,1024,128]{2,1,0:T(8,128)(2,1)S(1)}, u32[]{:S(2)}, u32[]{:S(2)}) collective-permute-start(bf16[4,1024,128]{2,1,0:T(8,128)(2,1)S(1)} %get-tuple-element.31.refs_0_), channel_id=1, source_target_pairs={{0,8},{8,16},{16,24},{24,0},{1,9},{9,17},{17,25},{25,1},{2,10},{10... | collective-permute-start | bytes 3145736 | tf_op jit(solution)/shard_map/ppermute | solution.py:31
  58.0 24.6 %collective-permute-start.17 = (bf16[4,512,128]{2,1,0:T(8,128)(2,1)S(1)}, bf16[4,512,128]{2,1,0:T(8,128)(2,1)S(1)}, u32[]{:S(2)}, u32[]{:S(2)}) collective-permute-start(bf16[4,512,128]{2,1,0:T(8,128)(2,1)S(1)} %get-tuple-element.26.refs_0_), channel_id=1, source_target_pairs={{0,24},{8,0},{16,8},{24,16},{1,25},{9,1},{17,9},{25,17},{2,26},{10... | collective-permute-start | bytes 1572872 | tf_op jit(solution)/shard_map/ppermute | solution.py:31
  87.9 33.1 %collective-permute-start.6 = (bf16[16,128,256]{2,1,0:T(8,128)(2,1)S(1)}, bf16[16,128,256]{2,1,0:T(8,128)(2,1)S(1)}, u32[]{:S(2)}, u32[]{:S(2)}) collective-permute-start(bf16[16,128,256]{2,1,0:T(8,128)(2,1)S(1)} %shard_map.165.refs_0_), channel_id=1, source_target_pairs={{0,1},{1,0},{2,3},{3,2},{4,5},{5,4},{6,7},{7,6},{8,9},{9,8},{10,11... | collective-permute-start | bytes 3145736 | tf_op jit(solution)/shard_map/ppermute | solution.py:35
  88.3 86.0 %collective-permute-start.25 = (bf16[12,128,1024]{2,1,0:T(8,128)(2,1)S(1)}, bf16[12,128,1024]{2,1,0:T(8,128)(2,1)}, u32[]{:S(2)}, u32[]{:S(2)}) collective-permute-start(bf16[12,128,1024]{2,1,0:T(8,128)(2,1)S(1)} %shard_map.173.refs_0_), channel_id=1, source_target_pairs={{0,1},{1,0},{2,3},{3,2},{4,5},{5,4},{6,7},{7,6},{8,9},{9,8},{10,11... | collective-permute-start | bytes 9437192 | tf_op jit(solution)/shard_map/ppermute | solution.py:35
  88.9 18.5 %collective-permute-start.8 = (bf16[2448,128]{1,0:T(8,128)(2,1)S(1)}, bf16[2448,128]{1,0:T(8,128)(2,1)S(1)}, u32[]{:S(2)}, u32[]{:S(2)}) collective-permute-start(bf16[2448,128]{1,0:T(8,128)(2,1)S(1)} %shard_map.166.refs_2_), channel_id=1, source_target_pairs={{0,4},{2,6},{4,0},{6,2},{1,5},{3,7},{5,1},{7,3},{8,12},{10,14},{12... | collective-permute-start | bytes 1880072 | tf_op jit(solution)/shard_map/ppermute | solution.py:31
  95.0 82.1 %collective-permute-start.31 = (bf16[12,1024,128]{2,1,0:T(8,128)(2,1)}, bf16[12,1024,128]{2,1,0:T(8,128)(2,1)}, u32[]{:S(2)}, u32[]{:S(2)}) collective-permute-start(bf16[12,1024,128]{2,1,0:T(8,128)(2,1)} %shard_map.177.refs_0_), channel_id=1, source_target_pairs={{0,1},{1,0},{2,3},{3,2},{4,5},{5,4},{6,7},{7,6},{8,9},{9,8},{10,11... | collective-permute-start | bytes 9437192 | tf_op jit(solution)/shard_map/ppermute | solution.py:35
  101.6 18.4 %collective-permute-start.9 = (bf16[2448,128]{1,0:T(8,128)(2,1)S(1)}, bf16[2448,128]{1,0:T(8,128)(2,1)S(1)}, u32[]{:S(2)}, u32[]{:S(2)}) collective-permute-start(bf16[2448,128]{1,0:T(8,128)(2,1)S(1)} %shard_map.166.refs_2_), channel_id=1, source_target_pairs={{0,2},{2,4},{4,6},{6,0},{1,3},{3,5},{5,7},{7,1},{8,10},{10,12},{12... | collective-permute-start | bytes 1880072 | tf_op jit(solution)/shard_map/ppermute | solution.py:31
  107.4 59.3 %collective-permute-start.20 = (bf16[16,512,128]{2,1,0:T(8,128)(2,1)}, bf16[16,512,128]{2,1,0:T(8,128)(2,1)}, u32[]{:S(2)}, u32[]{:S(2)}) collective-permute-start(bf16[16,512,128]{2,1,0:T(8,128)(2,1)} %shard_map.171.rest_0_), channel_id=1, source_target_pairs={{0,1},{1,0},{2,3},{3,2},{4,5},{5,4},{6,7},{7,6},{8,9},{9,8},{10,11... | collective-permute-start | bytes 6291464 | tf_op jit(solution)/shard_map/ppermute | solution.py:35
  121.1 16.1 %collective-permute-start.24 = (bf16[2,128,1024]{2,1,0:T(8,128)(2,1)S(1)}, bf16[2,128,1024]{2,1,0:T(8,128)(2,1)S(1)}, u32[]{:S(2)}, u32[]{:S(2)}) collective-permute-start(bf16[2,128,1024]{2,1,0:T(8,128)(2,1)S(1)} %get-tuple-element.30), channel_id=1, source_target_pairs={{0,224},{32,0},{64,32},{96,64},{128,96},{160,128},{192,160},{224,1... | collective-permute-start | bytes 1572872 | tf_op jit(solution)/shard_map/ppermute | solution.py:31
  152.1 19.8 %collective-permute-start.26 = (bf16[4,128,1024]{2,1,0:T(8,128)(2,1)S(1)}, bf16[4,128,1024]{2,1,0:T(8,128)(2,1)S(1)}, u32[]{:S(2)}, u32[]{:S(2)}) collective-permute-start(bf16[4,128,1024]{2,1,0:T(8,128)(2,1)S(1)} %shard_map.175.refs_1_), channel_id=1, source_target_pairs={{0,1},{1,0},{2,3},{3,2},{4,5},{5,4},{6,7},{7,6},{8,9},{9,8},{10,11... | collective-permute-start | bytes 3145736 | tf_op jit(solution)/shard_map/ppermute | solution.py:35
  153.6 23.5 %collective-permute-start.32 = (bf16[4,1024,128]{2,1,0:T(8,128)(2,1)S(1)}, bf16[4,1024,128]{2,1,0:T(8,128)(2,1)S(1)}, u32[]{:S(2)}, u32[]{:S(2)}) collective-permute-start(bf16[4,1024,128]{2,1,0:T(8,128)(2,1)S(1)} %shard_map.179.refs_1_), channel_id=1, source_target_pairs={{0,1},{1,0},{2,3},{3,2},{4,5},{5,4},{6,7},{7,6},{8,9},{9,8},{10,11... | collective-permute-start | bytes 3145736 | tf_op jit(solution)/shard_map/ppermute | solution.py:35
  171.0 16.4 %collective-permute-start.35 = (bf16[128,2048]{1,0:T(8,128)(2,1)S(1)}, bf16[128,2048]{1,0:T(8,128)(2,1)S(1)}, u32[]{:S(2)}, u32[]{:S(2)}) collective-permute-start(bf16[128,2048]{1,0:T(8,128)(2,1)S(1)} %get-tuple-element.34.refs_2_), channel_id=1, source_target_pairs={{0,4},{2,6},{4,0},{6,2},{1,5},{3,7},{5,1},{7,3},{8,12},{10,14},{12... | collective-permute-start | bytes 1572872 | tf_op jit(solution)/shard_map/ppermute | solution.py:31
  171.9 25.3 %collective-permute-start.33 = (bf16[128,2048]{1,0:T(8,128)(2,1)S(1)}, bf16[128,2048]{1,0:T(8,128)(2,1)S(1)}, u32[]{:S(2)}, u32[]{:S(2)}) collective-permute-start(bf16[128,2048]{1,0:T(8,128)(2,1)S(1)} %get-tuple-element.34.refs_2_), channel_id=1, source_target_pairs={{0,6},{2,0},{4,2},{6,4},{1,7},{3,1},{5,3},{7,5},{8,14},{10,8},{12,... | collective-permute-start | bytes 1572872 | tf_op jit(solution)/shard_map/ppermute | solution.py:31
  174.3 22.8 %collective-permute-start.34 = (bf16[128,2048]{1,0:T(8,128)(2,1)S(1)}, bf16[128,2048]{1,0:T(8,128)(2,1)S(1)}, u32[]{:S(2)}, u32[]{:S(2)}) collective-permute-start(bf16[128,2048]{1,0:T(8,128)(2,1)S(1)} %get-tuple-element.34.refs_2_), channel_id=1, source_target_pairs={{0,2},{2,4},{4,6},{6,0},{1,3},{3,5},{5,7},{7,1},{8,10},{10,12},{12... | collective-permute-start | bytes 1572872 | tf_op jit(solution)/shard_map/ppermute | solution.py:31
  (34 other events, 372.8 us)
where the time goes:
time: 222 us; the launch traced here: 220 us
  waiting for transfers between devices  105 us (47%)
  starting transfers between devices  53.3 us (24%)
  Pallas kernels  39.5 us (18%)
  blocking collectives  12.6 us (6%)
  local copies, waits for them, and re-layouts  8.42 us (4%)
    ppermute x33, waiting for transfers between devices, shift(): return lax.ppermute(x, axis, pairs)  105 us
    ppermute x33, starting transfers between devices, shift(): return lax.ppermute(x, axis, pairs)  51.8 us
    pallas_call x22, Pallas kernels, call(): pl.pallas_call(kernel, out_shape=[jax.ShapeDtypeStruct(s, d) for s, d in...  39.5 us
    all_to_all x1, blocking collectives, layer(): parts = lax.all_to_all(parts, 'y', 0, 0, tiled=True)  12.6 us
    unnamed x36, local copies, waits for them, and re-layouts  8.42 us
  transfers between devices with their start and end apart: 40, of which 18 were waited for; matrix products, arithmetic and copies ran while one was open for 0% of the time, Pallas kernels for 17%

commit v1 on v0

--- a/solution.py
+++ b/solution.py
@@ -49,13 +49,14 @@
 RAW = pl.BlockSpec(memory_space=pltpu.HBM)
 
 
-def call(kernel, outs, inputs, specs, scratch, out_specs=None, vmem=8):
+def call(kernel, outs, inputs, specs, scratch, out_specs=None, vmem=8, aliases={}):
     return pl.pallas_call(
         kernel,
         out_shape=[jax.ShapeDtypeStruct(s, d) for s, d in outs],
         in_specs=specs,
         out_specs=out_specs or [VM] * len(outs),
         scratch_shapes=scratch,
+        input_output_aliases=aliases,
         compiler_params=pltpu.CompilerParams(vmem_limit_bytes=vmem * 1024 * 1024),
     )(*inputs)
 
@@ -110,18 +111,11 @@
         at += width
 
 
-def merge_kernel(*refs):
-    sources, out, buffers, sem = refs[:2], refs[2], refs[3:5], refs[5]
+def rows_kernel(*refs):
+    sources, out, buffers, sem = refs[:4], refs[4], refs[5:9], refs[9]
     loaded(sources, buffers, sem)
-    out[...] = (buffers[0][...] * buffers[1][...]).astype(BF)
-
-
-def rows_kernel(m0, m1, m2, m3, weight, scale, out, weight_buffer, scale_buffer, sem):
-    started = copies([(weight, weight_buffer), (scale, scale_buffer)], sem)
-    for r, part in enumerate((m0, m1, m2, m3)):
-        out[r * T : (r + 1) * T] = part[...]
-    finish(started)
-    out[4 * T :] = (weight_buffer[...] * scale_buffer[...]).astype(BF)
+    out[:T] = (buffers[0][...] * buffers[1][...]).astype(BF)
+    out[T:] = (buffers[2][...] * buffers[3][...]).astype(BF)
 
 
 def split_columns_kernel(c0, c1, c2, c3, first, second):
@@ -173,6 +167,11 @@
 
 def halves_kernel(near, back, low, high, sem):
     finish(copies([(back.at[:2], low), (near.at[2:], high)], sem))
+
+
+def row_halves_kernel(near, back, low, high):
+    low[...] = back[:HALF]
+    high[...] = near[HALF:]
 
 
 def joined(arrays):
@@ -212,20 +211,27 @@
         out[lax.rem(idx[2] + g, 4)] = gelu(part).astype(BF)
 
 
-def mixer_kernel(idx, tokens, gain, parts, pack_own, pack_partner, *rest):
-    merges = rest[:2]
-    middle, normed, weight, gated, sem = rest[2:]
-    pairs = []
-    for q in range(2):
-        for zr in range(4):
-            for xr in range(4):
-                col = aligned(place_of(idx, zr, xr))
-                dst = weight.at[4 * q * T : 4 * (q + 1) * T, pl.ds(col, T)]
-                pairs.append((merges[q].at[4 * xr + zr], dst))
-    started = copies(pairs, sem)
-
-    def moments(y, sums):
-        value = [parts[y, :, (2 * q + 1) * T : (2 * q + 2) * T].astype(F32) for q in range(2)]
+def mixer_kernel(idx, *refs):
+    merges, middle, normed, sem = refs[5:7], refs[7], refs[8], refs[9]
+    tokens, gain, parts, pack_own, pack_partner, weight, gated, merge_sem = refs[10:]
+    small = copies(list(zip(refs[:5], (tokens, gain, parts, pack_own, pack_partner))), sem)
+
+    def placed(q, zr, xr, r):
+        col = aligned(place_of(idx, zr, xr))
+        dst = weight.at[pl.ds(aligned(4 * q + r), T), pl.ds(col, T)]
+        return pltpu.make_async_copy(merges[q].at[16 * r + 4 * xr + zr], dst, merge_sem)
+
+    places = [(q, zr, xr) for q in range(2) for zr in range(4) for xr in range(4)]
+
+    @pl.loop(0, 4)
+    def _(r):
+        for place in places:
+            placed(*place, r).start()
+
+    finish(small)
+
+    def moments(r, sums):
+        value = [parts[r, :, (2 * q + 1) * T : (2 * q + 2) * T].astype(F32) for q in range(2)]
         total = jnp.sum(value[0] + value[1], axis=1, keepdims=True)
         squares = jnp.sum(value[0] * value[0] + value[1] * value[1], axis=1, keepdims=True)
         return sums[0] + total, sums[1] + squares
@@ -255,7 +261,11 @@
             direct = parts[y, :, 2 * q * T : (2 * q + 1) * T].astype(F32)
             gated[:, pl.ds(pl.multiple_of((4 * q + r) * T, T), T)] = (direct * mixed).astype(BF)
 
-    finish(started)
+
+    @pl.loop(0, 4)
+    def _(r):
+        for place in places:
+            placed(*place, r).wait()
 
     @pl.loop(0, D // CHUNK)
     def _(n):
@@ -283,24 +293,35 @@
     finish(copies(pairs, sem))
 
 
-def down_kernel(idx, *refs):
-    out, sem = refs[4:]
+def down_place(out, at, q):
+    return out.at[q * FF_DEV : (q + 1) * FF_DEV, pl.ds(aligned(at), T)]
+
+
+def down_first_kernel(idx, *refs):
+    out, sem = refs[2:]
     pairs = []
     for q in range(2):
+        for n, xr in enumerate((0, 1, 3)):
+            for zr in range(4):
+                pairs.append((refs[q].at[4 * n + zr], down_place(out, place_of(idx, zr, xr), q)))
+    finish(copies(pairs, sem))
+
+
+def down_last_kernel(idx, own, partner, _, out, sem):
+    pairs = []
+    for q, source in enumerate((own, partner)):
         for zr in range(4):
-            for xr in range(4):
-                at = aligned(place_of(idx, zr, xr))
-                dst = out.at[q * FF_DEV : (q + 1) * FF_DEV, pl.ds(at, T)]
-                pairs.append((picked(refs[2 * q : 2 * q + 2], xr, zr), dst))
+            pairs.append((source.at[zr], down_place(out, place_of(idx, zr, 2), q)))
     finish(copies(pairs, sem))
 
 
-def ff_kernel(groups, up, down, *refs):
-    tokens = refs[:groups]
-    outs = refs[groups:-2]
+def ff_kernel(count, up, down, *refs):
+    tokens, outs = refs[:count], refs[count:-2]
     rows, hidden = refs[-2:]
-    for g, t in enumerate(tokens):
-        rows[g * T : (g + 1) * T] = t[...]
+    at = 0
+    for t in tokens:
+        rows[at : at + t.shape[0]] = t[...]
+        at += t.shape[0]
 
     @pl.loop(0, D // CHUNK)
     def _(n):
@@ -312,19 +333,19 @@
     def _(n):
         cols = pl.ds(pl.multiple_of(n * CHUNK, CHUNK), CHUNK)
         part = jnp.dot(hidden[...], down[:, cols], preferred_element_type=F32).astype(BF)
-        height = outs[0].shape[0]
+        size = outs[0].shape[0]
         for g, out in enumerate(outs):
-            out[:, cols] = part[g * height : (g + 1) * height]
-
-
-def ff(up, down, tokens, height=T):
-    groups = len(tokens)
+            out[:, cols] = part[g * size : (g + 1) * size]
+
+
+def ff(up, down, tokens, size=T):
+    height = sum(t.shape[0] for t in tokens)
     return call(
-        lambda *refs: ff_kernel(groups, *refs),
-        [((height, D), BF)] * (groups * T // height),
+        lambda *refs: ff_kernel(len(tokens), *refs),
+        [((size, D), BF)] * (height // size),
         (up, down, *tokens),
-        [VM] * (2 + groups),
-        [pltpu.VMEM((groups * T, D), BF), pltpu.VMEM((groups * T, D), BF)],
+        [VM] * (2 + len(tokens)),
+        [pltpu.VMEM((height, D), BF), pltpu.VMEM((height, D), BF)],
     )
 
 
@@ -365,8 +386,6 @@
 ):
     idx = jnp.stack([lax.axis_index(a) for a in ("z", "x", "y")]).astype(jnp.int32)
     row = lambda v: v.reshape(1, -1)
-    merge_half = prepared(merge_kernel, (T, T), (merge_weight, row(merge_scale)))
-    merge_y = others(merge_half, "y")
     columns = prepared(
         columns_kernel,
         (T, 2 * T + FF_DEV),
@@ -394,7 +413,9 @@
     )
     near_rows, far_rows, back_rows = others(normed, "y")
     rows = prepared(
-        rows_kernel, (4 * T + FF_DEV, T), (reduce_weight, row(reduce_scale)), (merge_half, *merge_y)
+        rows_kernel,
+        (T + FF_DEV, T),
+        (merge_weight, row(merge_scale), reduce_weight, row(reduce_scale)),
     )
     rows_z = (rows, *others(rows, ZRING))
     dv_stack, expand_stack = call(
@@ -403,9 +424,10 @@
     dv_own = joined((dv_stack, *others(dv_stack, ZRING)))
     dv_partner = swap(dv_own)
     merge_stack, reduce_stack = call(
-        split_rows_kernel, [((4, 4 * T, T), BF), ((4, FF_DEV, T), BF)], rows_z, [VM] * 4, []
-    )
-    merge_own = joined((merge_stack, *others(merge_stack, "x")))
+        split_rows_kernel, [((4, T, T), BF), ((4, FF_DEV, T), BF)], rows_z, [VM] * 4, []
+    )
+    merge_mine = joined((merge_stack, *others(merge_stack, "x")))
+    merge_own = joined((merge_mine, *others(merge_mine, "y")))
     merge_partner = swap(merge_own)
     expands = around(expand_stack, ZRING)
     reduces = around(reduce_stack, "x")
@@ -431,24 +453,46 @@
         [((T, D), BF), ((T, D), BF)],
         (
             idx,
-            tokens,
-            channel_gain.reshape(1, D),
+            pltpu.with_memory_space_constraint(tokens, pltpu.HBM),
+            pltpu.with_memory_space_constraint(row(channel_gain), pltpu.HBM),
             parts,
             pack_own,
             pack_partner,
             merge_own,
             merge_partner,
         ),
-        [SM] + [VM] * 5 + [HB] * 2,
-        [pltpu.VMEM((AW, D), BF), pltpu.VMEM((T, AW), BF), pltpu.SemaphoreType.DMA(())],
+        [SM] + [HB] * 7,
+        [
+            pltpu.SemaphoreType.DMA(()),
+            pltpu.VMEM((T, D), BF),
+            pltpu.VMEM((1, D), F32),
+            pltpu.VMEM((4, T, 4 * T), BF),
+            pltpu.VMEM((4, PACK, T), BF),
+            pltpu.VMEM((4, PACK, T), BF),
+            pltpu.VMEM((AW, D), BF),
+            pltpu.VMEM((T, AW), BF),
+            pltpu.SemaphoreType.DMA(()),
+        ],
         None,
         16,
     )
-    near_rows, far_rows, back_rows = others(normed, "y")
+    near_rows, back_rows = shift(normed, "y", -1), shift(normed, "y", 1)
+    low, high = call(row_halves_kernel, [((HALF, D), BF)] * 2, (near_rows, back_rows), [VM] * 2, [])
+    far_rows = shift(low, "y", 1), shift(high, "y", -1)
     dma = [pltpu.SemaphoreType.DMA(())]
     (up,) = call(up_kernel, [((D, 2 * FF_DEV), BF)], (idx, *expands), [SM] + [HB] * 4, dma)
-    (down,) = call(down_kernel, [((2 * FF_DEV, D), BF)], (idx, *reduces), [SM] + [HB] * 4, dma)
-    far_low, far_high = ff(up, down, (far_rows,), HALF)
+    whole = [((2 * FF_DEV, D), BF)]
+    near_own, far_own, near_partner, far_partner = reduces
+    (down,) = call(down_first_kernel, whole, (idx, near_own, near_partner), [SM, HB, HB], dma)
+    (down,) = call(
+        down_last_kernel,
+        whole,
+        (idx, far_own, far_partner, down),
+        [SM, HB, HB, VM],
+        dma,
+        aliases={3: 0},
+    )
+    far_low, far_high = ff(up, down, far_rows, HALF)
     near, back = ff(up, down, (near_rows, back_rows))
     (own,) = ff(up, down, (normed,))
     relay_low = shift(far_low, "y", 1)

time: 222 us -> 235 us (1.059)
  blocking collectives: 12.6 us -> 0 us
  waiting for transfers between devices: 105 us -> 116 us
  starting transfers between devices: 53.3 us -> 62.4 us
  Pallas kernels: 39.5 us -> 43.8 us
  local copies, waits for them, and re-layouts: 8.42 us -> 10.8 us
    all_to_all x1 -> x0, blocking collectives: 12.6 us -> none  [layer(): parts = lax.all_to_all(parts, 'y', 0, 0, tiled=True)]
    ppermute x33 -> x34, waiting for transfers between devices: 105 us -> 114 us  [shift(): return lax.ppermute(x, axis, pairs)]
    ppermute x33 -> x34, starting transfers between devices: 51.8 us -> 57.5 us  [shift(): return lax.ppermute(x, axis, pairs)]
    pallas_call x22 -> x24, Pallas kernels: 39.5 us -> 43.8 us  [call(): pl.pallas_call(kernel, out_shape=[jax.ShapeDtypeStruct(s, d) for s, d in...]
    all_to_all x0 -> x1, starting transfers between devices: none -> 4.15 us  [layer(): parts = lax.all_to_all(parts, 'y', 0, 0, tiled=True)]
    unnamed x36 -> x32, local copies, waits for them, and re-layouts: 8.42 us -> 10.8 us
  transfers between devices with their start and end apart: 40 -> 42, of which waited for: 18 -> 18; matrix products, arithmetic and copies ran while one was open for 0% -> 0% of each run, Pallas kernels for 17% -> 17%
where the time goes in v1:
time: 235 us; the launch traced here: 234 us
  waiting for transfers between devices  116 us (49%)
  starting transfers between devices  62.4 us (27%)
  Pallas kernels  43.8 us (19%)
  local copies, waits for them, and re-layouts  10.8 us (5%)
    ppermute x34, waiting for transfers between devices, shift(): return lax.ppermute(x, axis, pairs)  114 us
    ppermute x34, starting transfers between devices, shift(): return lax.ppermute(x, axis, pairs)  57.5 us
    pallas_call x24, Pallas kernels, call(): pl.pallas_call(kernel, out_shape=[jax.ShapeDtypeStruct(s, d) for s, d in...  43.8 us
    unnamed x32, local copies, waits for them, and re-layouts  10.8 us
  transfers between devices with their start and end apart: 42, of which 18 were waited for; matrix products, arithmetic and copies ran while one was open for 0% of the time, Pallas kernels for 17%

profile of v1, /device:TPU:2, one launch (start us, length us, event | category | flops | bytes accessed | tf_op | source)
XLA Modules:
  0.0 234.2 jit_solution(4256822181924627008)
XLA Ops:
  1.1 5.9 %collective-permute-start.11 = (bf16[1152,128]{1,0:T(8,128)(2,1)S(1)}, bf16[1152,128]{1,0:T(8,128)(2,1)S(1)}, u32[]{:S(2)}, u32[]{:S(2)}) collective-permute-start(bf16[1152,128]{1,0:T(8,128)(2,1)S(1)} %shard_map.168.r0), channel_id=1, source_target_pairs={{0,224},{32,0},{64,32},{96,64},{128,96},{160,128},{192,160},{224,1... | collective-permute-start | bytes 884744 | tf_op jit(solution)/shard_map/ppermute | solution.py:31
  9.5 10.1 %collective-permute-done.11.r1 = bf16[1152,128]{1,0:T(8,128)(2,1)S(1)} collective-permute-done((bf16[1152,128]{1,0:T(8,128)(2,1)S(1)}, bf16[1152,128]{1,0:T(8,128)(2,1)S(1)}, u32[]{:S(2)}, u32[]{:S(2)}) %collective-permute-start.11) | collective-permute-done | bytes 294944 | tf_op jit(solution)/shard_map/ppermute | solution.py:31
  19.7 3.4 %collective-permute-done.13.r3 = bf16[1152,128]{1,0:T(8,128)(2,1)S(1)} collective-permute-done((bf16[1152,128]{1,0:T(8,128)(2,1)S(1)}, bf16[1152,128]{1,0:T(8,128)(2,1)S(1)}, u32[]{:S(2)}, u32[]{:S(2)}) %collective-permute-start.13) | collective-permute-done | bytes 294944 | tf_op jit(solution)/shard_map/ppermute | solution.py:31
  40.2 5.4 %collective-permute-done.1.c2 = bf16[128,1280]{1,0:T(8,128)(2,1)S(1)} collective-permute-done((bf16[128,1280]{1,0:T(8,128)(2,1)S(1)}, bf16[128,1280]{1,0:T(8,128)(2,1)S(1)}, u32[]{:S(2)}, u32[]{:S(2)}) %collective-permute-start.1) | collective-permute-done | bytes 327712 | tf_op jit(solution)/shard_map/ppermute | solution.py:31
  59.2 7.4 %collective-permute-done.19.refs_3_ = bf16[16,128,128]{2,1,0:T(8,128)(2,1)S(1)} collective-permute-done((bf16[16,128,128]{2,1,0:T(8,128)(2,1)S(1)}, bf16[16,128,128]{2,1,0:T(8,128)(2,1)S(1)}, u32[]{:S(2)}, u32[]{:S(2)}) %collective-permute-start.19) | collective-permute-done | bytes 524320 | tf_op jit(solution)/shard_map/ppermute | solution.py:31
  68.9 16.7 %collective-permute-done.4.refs_2_ = bf16[4,128,256]{2,1,0:T(8,128)(2,1)S(1)} collective-permute-done((bf16[4,128,256]{2,1,0:T(8,128)(2,1)S(1)}, bf16[4,128,256]{2,1,0:T(8,128)(2,1)S(1)}, u32[]{:S(2)}, u32[]{:S(2)}) %collective-permute-start.4) | collective-permute-done | bytes 262176 | tf_op jit(solution)/shard_map/ppermute | solution.py:31
  94.9 8.1 %collective-permute-done.5.refs_3_ = bf16[4,128,256]{2,1,0:T(8,128)(2,1)S(1)} collective-permute-done((bf16[4,128,256]{2,1,0:T(8,128)(2,1)S(1)}, bf16[4,128,256]{2,1,0:T(8,128)(2,1)S(1)}, u32[]{:S(2)}, u32[]{:S(2)}) %collective-permute-start.5) | collective-permute-done | bytes 262176 | tf_op jit(solution)/shard_map/ppermute | solution.py:31
  104.2 13.2 %collective-permute-done.7.refs_3_ = bf16[2448,128]{1,0:T(8,128)(2,1)S(1)} collective-permute-done((bf16[2448,128]{1,0:T(8,128)(2,1)S(1)}, bf16[2448,128]{1,0:T(8,128)(2,1)S(1)}, u32[]{:S(2)}, u32[]{:S(2)}) %collective-permute-start.7) | collective-permute-done | bytes 626720 | tf_op jit(solution)/shard_map/ppermute | solution.py:31
  121.7 15.1 %collective-permute-done.9.refs_5_ = bf16[2448,128]{1,0:T(8,128)(2,1)S(1)} collective-permute-done((bf16[2448,128]{1,0:T(8,128)(2,1)S(1)}, bf16[2448,128]{1,0:T(8,128)(2,1)S(1)}, u32[]{:S(2)}, u32[]{:S(2)}) %collective-permute-start.9) | collective-permute-done | bytes 626720 | tf_op jit(solution)/shard_map/ppermute | solution.py:31
  144.4 4.7 %shard_map.167 = (bf16[4,128,512]{2,1,0:T(8,128)(2,1)S(1)}, bf16[4,400,128]{2,1,0:T(8,128)(2,1)S(1)}) custom-call(s32[3]{0:T(128)S(1)} %pad_add_fusion.idx, bf16[16,128,256]{2,1,0:T(8,128)(2,1)} %shard_map.165.refs_0_, bf16[16,128,256]{2,1,0:T(8,128)(2,1)} %collective-permute-done.6.refs_1_, bf16[2448,128]{1,0:T(8,128)(2,1)S(1)} %copy-done.5, ...), custom_call_target="tpu_custom_call" | custom-call | tf_op jit(solution)/shard_map/pallas_call | solution.py:53
  149.9 3.8 %collective-permute-done.29.refs_0_ = bf16[2,1024,128]{2,1,0:T(8,128)(2,1)} collective-permute-done((bf16[2,1024,128]{2,1,0:T(8,128)(2,1)}, bf16[2,1024,128]{2,1,0:T(8,128)(2,1)}, u32[]{:S(2)}, u32[]{:S(2)}) %collective-permute-start.29) | collective-permute-done | bytes 524320 | tf_op jit(solution)/shard_map/ppermute | solution.py:31
  156.6 4.1 %all-to-all-start = ((bf16[4,128,512]{2,1,0:T(8,128)(2,1)}), bf16[4,128,512]{2,1,0:T(8,128)(2,1)}, u32[]{:S(2)}, u32[]{:S(2)}) async-start(bf16[4,128,512]{2,1,0:T(8,128)(2,1)} %copy-done.12), calls=%async_computation | async-start | bytes 1048576 | tf_op jit(solution)/shard_map/all_to_all | solution.py:448
  164.4 3.2 %collective-permute-start.24 = (bf16[2,128,1024]{2,1,0:T(8,128)(2,1)}, bf16[2,128,1024]{2,1,0:T(8,128)(2,1)}, u32[]{:S(2)}, u32[]{:S(2)}) collective-permute-start(bf16[2,128,1024]{2,1,0:T(8,128)(2,1)} %get-tuple-element.32), channel_id=1, source_target_pairs={{0,224},{32,0},{64,32},{96,64},{128,96},{160,128},{192,160},{224,1... | collective-permute-start | bytes 1572872 | tf_op jit(solution)/shard_map/ppermute | solution.py:31
  170.2 4.9 %shard_map.172 = (bf16[128,2048]{1,0:T(8,128)(2,1)S(1)}, bf16[128,2048]{1,0:T(8,128)(2,1)S(1)}) custom-call(s32[3]{0:T(128)S(1)} %copy-done.14, bf16[128,2048]{1,0:T(8,128)(2,1)} %refs_0_.7, f32[1,2048]{1,0:T(1,128)} %bitcast.15, bf16[4,128,512]{2,1,0:T(8,128)(2,1)} %all-to-all-done.refs_2_, bf16[4,400,128]{2,1,0:T(8,128)(2,1)S(1)} %get-tuple-element.27.refs_3_, ...), custom_call_target="tpu_custom_call" | custom-call | tf_op jit(solution)/shard_map/pallas_call | solution.py:53
  180.4 6.6 %collective-permute-done.33.refs_2_.near = bf16[128,2048]{1,0:T(8,128)(2,1)S(1)} collective-permute-done((bf16[128,2048]{1,0:T(8,128)(2,1)S(1)}, bf16[128,2048]{1,0:T(8,128)(2,1)S(1)}, u32[]{:S(2)}, u32[]{:S(2)}) %collective-permute-start.33) | collective-permute-done | bytes 524320 | tf_op jit(solution)/shard_map/ppermute | solution.py:31
  187.5 11.4 %collective-permute-done.34.refs_3_.back = bf16[128,2048]{1,0:T(8,128)(2,1)S(1)} collective-permute-done((bf16[128,2048]{1,0:T(8,128)(2,1)S(1)}, bf16[128,2048]{1,0:T(8,128)(2,1)S(1)}, u32[]{:S(2)}, u32[]{:S(2)}) %collective-permute-start.34) | collective-permute-done | bytes 524320 | tf_op jit(solution)/shard_map/ppermute | solution.py:31
  199.0 3.2 %collective-permute-start.36 = (bf16[64,2048]{1,0:T(8,128)(2,1)S(1)}, bf16[64,2048]{1,0:T(8,128)(2,1)S(1)}, u32[]{:S(2)}, u32[]{:S(2)}) collective-permute-start(bf16[64,2048]{1,0:T(8,128)(2,1)S(1)} %get-tuple-element.40), channel_id=1, source_target_pairs={{0,6},{2,0},{4,2},{6,4},{1,7},{3,1},{5,3},{7,5},{8,14},{10,8},{12,... | collective-permute-start | bytes 786440 | tf_op jit(solution)/shard_map/ppermute | solution.py:31
  202.3 3.3 %shard_map.180._ = bf16[2048,2048]{1,0:T(8,128)(2,1)S(1)} custom-call(s32[3]{0:T(128)S(1)} %copy-done.15, bf16[12,1024,128]{2,1,0:T(8,128)(2,1)} %shard_map.179.refs_0_, bf16[12,1024,128]{2,1,0:T(8,128)(2,1)} %collective-permute-done.32.refs_1_), custom_call_target="tpu_custom_call" | custom-call | tf_op jit(solution)/shard_map/pallas_call | solution.py:53
  209.6 3.7 %shard_map.185 = (bf16[64,2048]{1,0:T(8,128)(2,1)S(1)}, bf16[64,2048]{1,0:T(8,128)(2,1)S(1)}) custom-call(bf16[2048,2048]{1,0:T(8,128)(2,1)S(1)} %shard_map.176.refs_0_, bf16[2048,2048]{1,0:T(8,128)(2,1)S(1)} %shard_map.181.refs_1_, bf16[64,2048]{1,0:T(8,128)(2,1)S(1)} %collective-permute-done.35.refs_2_, bf16[64,2048]{1,0:T(8,128)(2,1)S(1)} %collective-permute-done.36.refs_3_), custom_call_target="tpu_custom_call" | custom-call | tf_op jit(solution)/shard_map/pallas_call | solution.py:53
  213.4 3.2 %collective-permute-start.38 = (bf16[64,2048]{1,0:T(8,128)(2,1)S(1)}, bf16[64,2048]{1,0:T(8,128)(2,1)S(1)}, u32[]{:S(2)}, u32[]{:S(2)}) collective-permute-start(bf16[64,2048]{1,0:T(8,128)(2,1)S(1)} %get-tuple-element.42), channel_id=1, source_target_pairs={{0,6},{2,0},{4,2},{6,4},{1,7},{3,1},{5,3},{7,5},{8,14},{10,8},{12,... | collective-permute-start | bytes 786440 | tf_op jit(solution)/shard_map/ppermute | solution.py:31
  216.6 5.8 %shard_map.183 = (bf16[128,2048]{1,0:T(8,128)(2,1)S(1)}, bf16[128,2048]{1,0:T(8,128)(2,1)S(1)}) custom-call(bf16[2048,2048]{1,0:T(8,128)(2,1)S(1)} %shard_map.176.refs_0_, bf16[2048,2048]{1,0:T(8,128)(2,1)S(1)} %shard_map.181.refs_1_, bf16[128,2048]{1,0:T(8,128)(2,1)S(1)} %collective-permute-done.33.refs_2_.near, ...), custom_call_target="tpu_custom_call" | custom-call | tf_op jit(solution)/shard_map/pallas_call | solution.py:53
  222.7 3.2 %collective-permute-start.40 = (bf16[128,2048]{1,0:T(8,128)(2,1)S(1)}, bf16[128,2048]{1,0:T(8,128)(2,1)S(1)}, u32[]{:S(2)}, u32[]{:S(2)}) collective-permute-start(bf16[128,2048]{1,0:T(8,128)(2,1)S(1)} %get-tuple-element.44), channel_id=1, source_target_pairs={{0,6},{2,0},{4,2},{6,4},{1,7},{3,1},{5,3},{7,5},{8,14},{10,8},{12,... | collective-permute-start | bytes 1572872 | tf_op jit(solution)/shard_map/ppermute | solution.py:31
  225.9 3.7 %shard_map.182 = bf16[128,2048]{1,0:T(8,128)(2,1)S(1)} custom-call(bf16[2048,2048]{1,0:T(8,128)(2,1)S(1)} %shard_map.176.refs_0_, bf16[2048,2048]{1,0:T(8,128)(2,1)S(1)} %shard_map.181.refs_1_, bf16[128,2048]{1,0:T(8,128)(2,1)S(1)} %get-tuple-element.36.refs_2_), custom_call_target="tpu_custom_call" | custom-call | tf_op jit(solution)/shard_map/pallas_call | solution.py:53
  229.6 3.4 %collective-permute-done.39 = bf16[128,2048]{1,0:T(8,128)(2,1)S(1)} collective-permute-done((bf16[128,2048]{1,0:T(8,128)(2,1)S(1)}, bf16[128,2048]{1,0:T(8,128)(2,1)S(1)}, u32[]{:S(2)}, u32[]{:S(2)}) %collective-permute-start.39) | collective-permute-done | bytes 524320 | tf_op jit(solution)/shard_map/ppermute | solution.py:31
  (118 shorter events, 80.0 us)
Async XLA Ops:
  1.1 18.5 %collective-permute-start.11 = (bf16[1152,128]{1,0:T(8,128)(2,1)S(1)}, bf16[1152,128]{1,0:T(8,128)(2,1)S(1)}, u32[]{:S(2)}, u32[]{:S(2)}) collective-permute-start(bf16[1152,128]{1,0:T(8,128)(2,1)S(1)} %shard_map.168.r0), channel_id=1, source_target_pairs={{0,224},{32,0},{64,32},{96,64},{128,96},{160,128},{192,160},{224,1... | collective-permute-start | bytes 884744 | tf_op jit(solution)/shard_map/ppermute | solution.py:31
  7.1 16.0 %collective-permute-start.13 = (bf16[1152,128]{1,0:T(8,128)(2,1)S(1)}, bf16[1152,128]{1,0:T(8,128)(2,1)S(1)}, u32[]{:S(2)}, u32[]{:S(2)}) collective-permute-start(bf16[1152,128]{1,0:T(8,128)(2,1)S(1)} %shard_map.168.r0), channel_id=1, source_target_pairs={{0,32},{32,64},{64,96},{96,128},{128,160},{160,192},{192,224},{224... | collective-permute-start | bytes 884744 | tf_op jit(solution)/shard_map/ppermute | solution.py:31
  29.5 16.1 %collective-permute-start.1 = (bf16[128,1280]{1,0:T(8,128)(2,1)S(1)}, bf16[128,1280]{1,0:T(8,128)(2,1)S(1)}, u32[]{:S(2)}, u32[]{:S(2)}) collective-permute-start(bf16[128,1280]{1,0:T(8,128)(2,1)S(1)} %shard_map.163.c0), channel_id=1, source_target_pairs={{0,16},{8,24},{16,0},{24,8},{1,17},{9,25},{17,1},{25,9},{2,18},{10... | collective-permute-start | bytes 983048 | tf_op jit(solution)/shard_map/ppermute | solution.py:31
  30.8 15.7 %collective-permute-start.2 = (bf16[128,1280]{1,0:T(8,128)(2,1)S(1)}, bf16[128,1280]{1,0:T(8,128)(2,1)S(1)}, u32[]{:S(2)}, u32[]{:S(2)}) collective-permute-start(bf16[128,1280]{1,0:T(8,128)(2,1)S(1)} %shard_map.163.c0), channel_id=1, source_target_pairs={{0,8},{8,16},{16,24},{24,0},{1,9},{9,17},{17,25},{25,1},{2,10},{10... | collective-permute-start | bytes 983048 | tf_op jit(solution)/shard_map/ppermute | solution.py:31
  34.0 23.1 %collective-permute-start.17 = (bf16[16,128,128]{2,1,0:T(8,128)(2,1)S(1)}, bf16[16,128,128]{2,1,0:T(8,128)(2,1)S(1)}, u32[]{:S(2)}, u32[]{:S(2)}) collective-permute-start(bf16[16,128,128]{2,1,0:T(8,128)(2,1)S(1)} %shard_map.170.refs_0_), channel_id=1, source_target_pairs={{0,6},{2,0},{4,2},{6,4},{1,7},{3,1},{5,3},{7,5},{8,14},{10,8},{12,... | collective-permute-start | bytes 1572872 | tf_op jit(solution)/shard_map/ppermute | solution.py:31
  37.1 21.2 %collective-permute-start.18 = (bf16[16,128,128]{2,1,0:T(8,128)(2,1)S(1)}, bf16[16,128,128]{2,1,0:T(8,128)(2,1)S(1)}, u32[]{:S(2)}, u32[]{:S(2)}) collective-permute-start(bf16[16,128,128]{2,1,0:T(8,128)(2,1)S(1)} %shard_map.170.refs_0_), channel_id=1, source_target_pairs={{0,4},{2,6},{4,0},{6,2},{1,5},{3,7},{5,1},{7,3},{8,12},{10,14},{12... | collective-permute-start | bytes 1572872 | tf_op jit(solution)/shard_map/ppermute | solution.py:31
  47.7 39.2 %collective-permute-start.27 = (bf16[4,1024,128]{2,1,0:T(8,128)(2,1)S(1)}, bf16[4,1024,128]{2,1,0:T(8,128)(2,1)S(1)}, u32[]{:S(2)}, u32[]{:S(2)}) collective-permute-start(bf16[4,1024,128]{2,1,0:T(8,128)(2,1)S(1)} %get-tuple-element.33.refs_0_), channel_id=1, source_target_pairs={{0,24},{8,0},{16,8},{24,16},{1,25},{9,1},{17,9},{25,17},{2,26},{10... | collective-permute-start | bytes 3145736 | tf_op jit(solution)/shard_map/ppermute | solution.py:31
  50.4 39.4 %collective-permute-start.28 = (bf16[4,1024,128]{2,1,0:T(8,128)(2,1)S(1)}, bf16[4,1024,128]{2,1,0:T(8,128)(2,1)S(1)}, u32[]{:S(2)}, u32[]{:S(2)}) collective-permute-start(bf16[4,1024,128]{2,1,0:T(8,128)(2,1)S(1)} %get-tuple-element.33.refs_0_), channel_id=1, source_target_pairs={{0,8},{8,16},{16,24},{24,0},{1,9},{9,17},{17,25},{25,1},{2,10},{10... | collective-permute-start | bytes 3145736 | tf_op jit(solution)/shard_map/ppermute | solution.py:31
  57.1 36.5 %collective-permute-start.21 = (bf16[4,128,1024]{2,1,0:T(8,128)(2,1)S(1)}, bf16[4,128,1024]{2,1,0:T(8,128)(2,1)S(1)}, u32[]{:S(2)}, u32[]{:S(2)}) collective-permute-start(bf16[4,128,1024]{2,1,0:T(8,128)(2,1)S(1)} %get-tuple-element.30.refs_0_), channel_id=1, source_target_pairs={{0,224},{32,0},{64,32},{96,64},{128,96},{160,128},{192,160},{224,1... | collective-permute-start | bytes 3145736 | tf_op jit(solution)/shard_map/ppermute | solution.py:31
  58.3 35.5 %collective-permute-start.22 = (bf16[4,128,1024]{2,1,0:T(8,128)(2,1)S(1)}, bf16[4,128,1024]{2,1,0:T(8,128)(2,1)S(1)}, u32[]{:S(2)}, u32[]{:S(2)}) collective-permute-start(bf16[4,128,1024]{2,1,0:T(8,128)(2,1)S(1)} %get-tuple-element.30.refs_0_), channel_id=1, source_target_pairs={{0,32},{32,64},{64,96},{96,128},{128,160},{160,192},{192,224},{224... | collective-permute-start | bytes 3145736 | tf_op jit(solution)/shard_map/ppermute | solution.py:31
  66.6 19.0 %collective-permute-start.4 = (bf16[4,128,256]{2,1,0:T(8,128)(2,1)S(1)}, bf16[4,128,256]{2,1,0:T(8,128)(2,1)S(1)}, u32[]{:S(2)}, u32[]{:S(2)}) collective-permute-start(bf16[4,128,256]{2,1,0:T(8,128)(2,1)S(1)} %get-tuple-element.25.refs_0_), channel_id=1, source_target_pairs={{0,64},{32,224},{64,128},{96,32},{128,192},{160,96},{192,0},{224,1... | collective-permute-start | bytes 786440 | tf_op jit(solution)/shard_map/ppermute | solution.py:31
  85.6 78.8 %collective-permute-start.20 = (bf16[64,128,128]{2,1,0:T(8,128)(2,1)}, bf16[64,128,128]{2,1,0:T(8,128)(2,1)}, u32[]{:S(2)}, u32[]{:S(2)}) collective-permute-start(bf16[64,128,128]{2,1,0:T(8,128)(2,1)} %shard_map.171.refs_5_), channel_id=1, source_target_pairs={{0,1},{1,0},{2,3},{3,2},{4,5},{5,4},{6,7},{7,6},{8,9},{9,8},{10,11... | collective-permute-start | bytes 6291464 | tf_op jit(solution)/shard_map/ppermute | solution.py:35
  86.9 30.4 %collective-permute-start.7 = (bf16[2448,128]{1,0:T(8,128)(2,1)S(1)}, bf16[2448,128]{1,0:T(8,128)(2,1)S(1)}, u32[]{:S(2)}, u32[]{:S(2)}) collective-permute-start(bf16[2448,128]{1,0:T(8,128)(2,1)S(1)} %shard_map.166.refs_2_), channel_id=1, source_target_pairs={{0,6},{2,0},{4,2},{6,4},{1,7},{3,1},{5,3},{7,5},{8,14},{10,8},{12,... | collective-permute-start | bytes 1880072 | tf_op jit(solution)/shard_map/ppermute | solution.py:31
  89.9 28.3 %collective-permute-start.8 = (bf16[2448,128]{1,0:T(8,128)(2,1)S(1)}, bf16[2448,128]{1,0:T(8,128)(2,1)S(1)}, u32[]{:S(2)}, u32[]{:S(2)}) collective-permute-start(bf16[2448,128]{1,0:T(8,128)(2,1)S(1)} %shard_map.166.refs_2_), channel_id=1, source_target_pairs={{0,4},{2,6},{4,0},{6,2},{1,5},{3,7},{5,1},{7,3},{8,12},{10,14},{12... | collective-permute-start | bytes 1880072 | tf_op jit(solution)/shard_map/ppermute | solution.py:31
  93.8 105.3 %collective-permute-start.32 = (bf16[12,1024,128]{2,1,0:T(8,128)(2,1)}, bf16[12,1024,128]{2,1,0:T(8,128)(2,1)}, u32[]{:S(2)}, u32[]{:S(2)}) collective-permute-start(bf16[12,1024,128]{2,1,0:T(8,128)(2,1)} %shard_map.179.refs_0_), channel_id=1, source_target_pairs={{0,1},{1,0},{2,3},{3,2},{4,5},{5,4},{6,7},{7,6},{8,9},{9,8},{10,11... | collective-permute-start | bytes 9437192 | tf_op jit(solution)/shard_map/ppermute | solution.py:35
  103.1 103.7 %collective-permute-start.25 = (bf16[12,128,1024]{2,1,0:T(8,128)(2,1)S(1)}, bf16[12,128,1024]{2,1,0:T(8,128)(2,1)}, u32[]{:S(2)}, u32[]{:S(2)}) collective-permute-start(bf16[12,128,1024]{2,1,0:T(8,128)(2,1)S(1)} %shard_map.173.refs_0_), channel_id=1, source_target_pairs={{0,1},{1,0},{2,3},{3,2},{4,5},{5,4},{6,7},{7,6},{8,9},{9,8},{10,11... | collective-permute-start | bytes 9437192 | tf_op jit(solution)/shard_map/ppermute | solution.py:35
  118.2 21.9 %collective-permute-start.6 = (bf16[16,128,256]{2,1,0:T(8,128)(2,1)}, bf16[16,128,256]{2,1,0:T(8,128)(2,1)}, u32[]{:S(2)}, u32[]{:S(2)}) collective-permute-start(bf16[16,128,256]{2,1,0:T(8,128)(2,1)} %shard_map.165.refs_0_), channel_id=1, source_target_pairs={{0,1},{1,0},{2,3},{3,2},{4,5},{5,4},{6,7},{7,6},{8,9},{9,8},{10,11... | collective-permute-start | bytes 3145736 | tf_op jit(solution)/shard_map/ppermute | solution.py:35
  118.2 18.5 %collective-permute-start.9 = (bf16[2448,128]{1,0:T(8,128)(2,1)S(1)}, bf16[2448,128]{1,0:T(8,128)(2,1)S(1)}, u32[]{:S(2)}, u32[]{:S(2)}) collective-permute-start(bf16[2448,128]{1,0:T(8,128)(2,1)S(1)} %shard_map.166.refs_2_), channel_id=1, source_target_pairs={{0,2},{2,4},{4,6},{6,0},{1,3},{3,5},{5,7},{7,1},{8,10},{10,12},{12... | collective-permute-start | bytes 1880072 | tf_op jit(solution)/shard_map/ppermute | solution.py:31
  137.6 16.1 %collective-permute-start.29 = (bf16[2,1024,128]{2,1,0:T(8,128)(2,1)}, bf16[2,1024,128]{2,1,0:T(8,128)(2,1)}, u32[]{:S(2)}, u32[]{:S(2)}) collective-permute-start(bf16[2,1024,128]{2,1,0:T(8,128)(2,1)} %get-tuple-element.34), channel_id=1, source_target_pairs={{0,8},{8,16},{16,24},{24,0},{1,9},{9,17},{17,25},{25,1},{2,10},{10... | collective-permute-start | bytes 1572872 | tf_op jit(solution)/shard_map/ppermute | solution.py:31
  149.9 14.5 %collective-permute-start.10 = (bf16[4,400,128]{2,1,0:T(8,128)(2,1)S(1)}, bf16[4,400,128]{2,1,0:T(8,128)(2,1)}, u32[]{:S(2)}, u32[]{:S(2)}) collective-permute-start(bf16[4,400,128]{2,1,0:T(8,128)(2,1)S(1)} %get-tuple-element.27.refs_3_), channel_id=1, source_target_pairs={{0,1},{1,0},{2,3},{3,2},{4,5},{5,4},{6,7},{7,6},{8,9},{9,8},{10,11... | collective-permute-start | bytes 1228808 | tf_op jit(solution)/shard_map/ppermute | solution.py:35
  153.7 21.5 %collective-permute-start.30 = (bf16[2,1024,128]{2,1,0:T(8,128)(2,1)}, bf16[2,1024,128]{2,1,0:T(8,128)(2,1)}, u32[]{:S(2)}, u32[]{:S(2)}) collective-permute-start(bf16[2,1024,128]{2,1,0:T(8,128)(2,1)} %get-tuple-element.35), channel_id=1, source_target_pairs={{0,24},{8,0},{16,8},{24,16},{1,25},{9,1},{17,9},{25,17},{2,26},{10... | collective-permute-start | bytes 1572872 | tf_op jit(solution)/shard_map/ppermute | solution.py:31
  164.3 14.2 %collective-permute-start.23 = (bf16[2,128,1024]{2,1,0:T(8,128)(2,1)}, bf16[2,128,1024]{2,1,0:T(8,128)(2,1)}, u32[]{:S(2)}, u32[]{:S(2)}) collective-permute-start(bf16[2,128,1024]{2,1,0:T(8,128)(2,1)} %get-tuple-element.31), channel_id=1, source_target_pairs={{0,32},{32,64},{64,96},{96,128},{128,160},{160,192},{192,224},{224... | collective-permute-start | bytes 1572872 | tf_op jit(solution)/shard_map/ppermute | solution.py:31
  178.5 27.0 %collective-permute-start.31 = (bf16[4,1024,128]{2,1,0:T(8,128)(2,1)S(1)}, bf16[4,1024,128]{2,1,0:T(8,128)(2,1)S(1)}, u32[]{:S(2)}, u32[]{:S(2)}) collective-permute-start(bf16[4,1024,128]{2,1,0:T(8,128)(2,1)S(1)} %shard_map.178.own), channel_id=1, source_target_pairs={{0,1},{1,0},{2,3},{3,2},{4,5},{5,4},{6,7},{7,6},{8,9},{9,8},{10,11... | collective-permute-start | bytes 3145736 | tf_op jit(solution)/shard_map/ppermute | solution.py:35
  179.8 27.0 %collective-permute-start.26 = (bf16[4,128,1024]{2,1,0:T(8,128)(2,1)S(1)}, bf16[4,128,1024]{2,1,0:T(8,128)(2,1)S(1)}, u32[]{:S(2)}, u32[]{:S(2)}) collective-permute-start(bf16[4,128,1024]{2,1,0:T(8,128)(2,1)S(1)} %shard_map.175.refs_1_), channel_id=1, source_target_pairs={{0,1},{1,0},{2,3},{3,2},{4,5},{5,4},{6,7},{7,6},{8,9},{9,8},{10,11... | collective-permute-start | bytes 3145736 | tf_op jit(solution)/shard_map/ppermute | solution.py:35
  (34 other events, 286.3 us)

commit v2 on v1

--- a/solution.py
+++ b/solution.py
@@ -212,21 +212,23 @@
 
 
 def mixer_kernel(idx, *refs):
-    merges, middle, normed, sem = refs[5:7], refs[7], refs[8], refs[9]
-    tokens, gain, parts, pack_own, pack_partner, weight, gated, merge_sem = refs[10:]
+    merges, middle, normed, sem = refs[5:9], refs[9], refs[10], refs[11]
+    tokens, gain, parts, pack_own, pack_partner, weight, gated, merge_sem = refs[12:]
     small = copies(list(zip(refs[:5], (tokens, gain, parts, pack_own, pack_partner))), sem)
 
-    def placed(q, zr, xr, r):
-        col = aligned(place_of(idx, zr, xr))
-        dst = weight.at[pl.ds(aligned(4 * q + r), T), pl.ds(col, T)]
-        return pltpu.make_async_copy(merges[q].at[16 * r + 4 * xr + zr], dst, merge_sem)
-
-    places = [(q, zr, xr) for q in range(2) for zr in range(4) for xr in range(4)]
-
-    @pl.loop(0, 4)
-    def _(r):
-        for place in places:
-            placed(*place, r).start()
+    def placed(n, q, r):
+        zr, xr = lax.div(n, 4), lax.rem(n, 4)
+        source = merges[2 * q + min(r, 1)].at[16 * max(r - 1, 0) + 4 * xr + zr]
+        at = (4 * q + r) * T
+        dst = weight.at[at : at + T, pl.ds(aligned(place_of(idx, zr, xr)), T)]
+        return pltpu.make_async_copy(source, dst, merge_sem)
+
+    pieces = [(q, r) for q in range(2) for r in range(4)]
+
+    @pl.loop(0, 16)
+    def _(n):
+        for piece in pieces:
+            placed(n, *piece).start()
 
     finish(small)
 
@@ -262,10 +264,10 @@
             gated[:, pl.ds(pl.multiple_of((4 * q + r) * T, T), T)] = (direct * mixed).astype(BF)
 
 
-    @pl.loop(0, 4)
-    def _(r):
-        for place in places:
-            placed(*place, r).wait()
+    @pl.loop(0, 16)
+    def _(n):
+        for piece in pieces:
+            placed(n, *piece).wait()
 
     @pl.loop(0, D // CHUNK)
     def _(n):
@@ -276,21 +278,26 @@
     normed[...] = rms(middle[...].astype(F32), gain[...]).astype(BF)
 
 
-def picked(parts, n, k):
-    near, far = parts
-    return far.at[k] if n == 2 else near.at[(0, 4, None, 8)[n] + k]
-
-
 def up_kernel(idx, *refs):
     out, sem = refs[4:]
-    pairs = []
-    for q in range(2):
-        for zr in range(4):
-            for xr in range(4):
-                at = aligned(place_of(idx, zr, xr))
-                dst = out.at[pl.ds(at, T), q * FF_DEV : (q + 1) * FF_DEV]
-                pairs.append((picked(refs[2 * q : 2 * q + 2], zr, xr), dst))
-    finish(copies(pairs, sem))
+
+    def placed(xr, q, zr):
+        dst = out.at[pl.ds(aligned(place_of(idx, zr, xr)), T), q * FF_DEV : (q + 1) * FF_DEV]
+        near, far = refs[2 * q : 2 * q + 2]
+        source = far.at[xr] if zr == 2 else near.at[(0, 4, None, 8)[zr] + xr]
+        return pltpu.make_async_copy(source, dst, sem)
+
+    pieces = [(q, zr) for q in range(2) for zr in range(4)]
+
+    @pl.loop(0, 4)
+    def _(xr):
+        for piece in pieces:
+            placed(xr, *piece).start()
+
+    @pl.loop(0, 4)
+    def _(xr):
+        for piece in pieces:
+            placed(xr, *piece).wait()
 
 
 def down_place(out, at, q):
@@ -299,12 +306,22 @@
 
 def down_first_kernel(idx, *refs):
     out, sem = refs[2:]
-    pairs = []
-    for q in range(2):
-        for n, xr in enumerate((0, 1, 3)):
-            for zr in range(4):
-                pairs.append((refs[q].at[4 * n + zr], down_place(out, place_of(idx, zr, xr), q)))
-    finish(copies(pairs, sem))
+
+    def placed(zr, q, n):
+        dst = down_place(out, place_of(idx, zr, (0, 1, 3)[n]), q)
+        return pltpu.make_async_copy(refs[q].at[4 * n + zr], dst, sem)
+
+    pieces = [(q, n) for q in range(2) for n in range(3)]
+
+    @pl.loop(0, 4)
+    def _(zr):
+        for piece in pieces:
+            placed(zr, *piece).start()
+
+    @pl.loop(0, 4)
+    def _(zr):
+        for piece in pieces:
+            placed(zr, *piece).wait()
 
 
 def down_last_kernel(idx, own, partner, _, out, sem):
@@ -427,8 +444,8 @@
         split_rows_kernel, [((4, T, T), BF), ((4, FF_DEV, T), BF)], rows_z, [VM] * 4, []
     )
     merge_mine = joined((merge_stack, *others(merge_stack, "x")))
-    merge_own = joined((merge_mine, *others(merge_mine, "y")))
-    merge_partner = swap(merge_own)
+    merge_rest = joined(others(merge_mine, "y"))
+    merges = (merge_mine, merge_rest, swap(merge_mine), swap(merge_rest))
     expands = around(expand_stack, ZRING)
     reduces = around(reduce_stack, "x")
 
@@ -458,10 +475,9 @@
             parts,
             pack_own,
             pack_partner,
-            merge_own,
-            merge_partner,
+            *merges,
         ),
-        [SM] + [HB] * 7,
+        [SM] + [HB] * 9,
         [
             pltpu.SemaphoreType.DMA(()),
             pltpu.VMEM((T, D), BF),

time: 235 us -> 219 us (0.932); the launches traced: 234 us -> 215 us
  waiting for transfers between devices: 116 us -> 91.6 us
  starting transfers between devices: 62.4 us -> 65.8 us
    ppermute x34, waiting for transfers between devices: 114 us -> 89.2 us  [shift(): return lax.ppermute(x, axis, pairs)]
    unnamed x32 -> x40, local copies, waits for them, and re-layouts: 10.8 us -> 12.2 us
  transfers between devices with their start and end apart: 42 -> 43, of which waited for: 18 -> 17; matrix products, arithmetic and copies ran while one was open for 0% -> 0% of each run, Pallas kernels for 17% -> 18%
where the time goes in v2:
time: 219 us; the launch traced here: 215 us
  waiting for transfers between devices  91.6 us (42%)
  starting transfers between devices  65.8 us (30%)
  Pallas kernels  43.7 us (20%)
  local copies, waits for them, and re-layouts  12.2 us (6%)
    ppermute x34, waiting for transfers between devices, shift(): return lax.ppermute(x, axis, pairs)  89.2 us
    ppermute x34, starting transfers between devices, shift(): return lax.ppermute(x, axis, pairs)  59.7 us
    pallas_call x24, Pallas kernels, call(): pl.pallas_call(kernel, out_shape=[jax.ShapeDtypeStruct(s, d) for s, d in...  43.7 us
    unnamed x40, local copies, waits for them, and re-layouts  12.2 us
  transfers between devices with their start and end apart: 43, of which 17 were waited for; matrix products, arithmetic and copies ran while one was open for 0% of the time, Pallas kernels for 18%

profile of v2, /device:TPU:2, one launch (start us, length us, event | category | flops | bytes accessed | tf_op | source)
XLA Modules:
  0.0 214.9 jit_solution(2128604895253183947)
XLA Ops:
  7.2 5.9 %collective-permute-start.11 = (bf16[1152,128]{1,0:T(8,128)(2,1)S(1)}, bf16[1152,128]{1,0:T(8,128)(2,1)S(1)}, u32[]{:S(2)}, u32[]{:S(2)}) collective-permute-start(bf16[1152,128]{1,0:T(8,128)(2,1)S(1)} %shard_map.168.r0), channel_id=1, source_target_pairs={{0,224},{32,0},{64,32},{96,64},{128,96},{160,128},{192,160},{224,1... | collective-permute-start | bytes 884744 | tf_op jit(solution)/shard_map/ppermute | solution.py:31
  19.7 5.9 %collective-permute-start.3 = (bf16[4,128,256]{2,1,0:T(8,128)(2,1)S(1)}, bf16[4,128,256]{2,1,0:T(8,128)(2,1)S(1)}, u32[]{:S(2)}, u32[]{:S(2)}) collective-permute-start(bf16[4,128,256]{2,1,0:T(8,128)(2,1)S(1)} %get-tuple-element.25.refs_0_), channel_id=1, source_target_pairs={{0,224},{32,0},{64,32},{96,64},{128,96},{160,128},{192,160},{224,1... | collective-permute-start | bytes 786440 | tf_op jit(solution)/shard_map/ppermute | solution.py:31
  25.6 3.4 %collective-permute-done.13.r3 = bf16[1152,128]{1,0:T(8,128)(2,1)S(1)} collective-permute-done((bf16[1152,128]{1,0:T(8,128)(2,1)S(1)}, bf16[1152,128]{1,0:T(8,128)(2,1)S(1)}, u32[]{:S(2)}, u32[]{:S(2)}) %collective-permute-start.13) | collective-permute-done | bytes 294944 | tf_op jit(solution)/shard_map/ppermute | solution.py:31
  29.6 3.8 %collective-permute-start.15 = (bf16[4,128,128]{2,1,0:T(8,128)(2,1)S(1)}, bf16[4,128,128]{2,1,0:T(8,128)(2,1)S(1)}, u32[]{:S(2)}, u32[]{:S(2)}) collective-permute-start(bf16[4,128,128]{2,1,0:T(8,128)(2,1)S(1)} %get-tuple-element.28.refs_0_), channel_id=1, source_target_pairs={{0,16},{8,24},{16,0},{24,8},{1,17},{9,25},{17,1},{25,9},{2,18},{10... | collective-permute-start | bytes 393224 | tf_op jit(solution)/shard_map/ppermute | solution.py:31
  50.4 6.3 %collective-permute-done.4.refs_2_ = bf16[4,128,256]{2,1,0:T(8,128)(2,1)S(1)} collective-permute-done((bf16[4,128,256]{2,1,0:T(8,128)(2,1)S(1)}, bf16[4,128,256]{2,1,0:T(8,128)(2,1)S(1)}, u32[]{:S(2)}, u32[]{:S(2)}) %collective-permute-start.4) | collective-permute-done | bytes 262176 | tf_op jit(solution)/shard_map/ppermute | solution.py:31
  60.0 3.9 %collective-permute-done.17.refs_0_ = bf16[16,128,128]{2,1,0:T(8,128)(2,1)S(1)} collective-permute-done((bf16[16,128,128]{2,1,0:T(8,128)(2,1)}, bf16[16,128,128]{2,1,0:T(8,128)(2,1)S(1)}, u32[]{:S(2)}, u32[]{:S(2)}) %collective-permute-start.17) | collective-permute-done | bytes 524320 | tf_op jit(solution)/shard_map/ppermute | solution.py:31
  65.3 13.6 %collective-permute-done.19.refs_2_ = bf16[16,128,128]{2,1,0:T(8,128)(2,1)S(1)} collective-permute-done((bf16[16,128,128]{2,1,0:T(8,128)(2,1)}, bf16[16,128,128]{2,1,0:T(8,128)(2,1)S(1)}, u32[]{:S(2)}, u32[]{:S(2)}) %collective-permute-start.19) | collective-permute-done | bytes 524320 | tf_op jit(solution)/shard_map/ppermute | solution.py:31
  78.9 3.5 %collective-permute-start.7 = (bf16[2448,128]{1,0:T(8,128)(2,1)S(1)}, bf16[2448,128]{1,0:T(8,128)(2,1)S(1)}, u32[]{:S(2)}, u32[]{:S(2)}) collective-permute-start(bf16[2448,128]{1,0:T(8,128)(2,1)S(1)} %shard_map.166.refs_2_), channel_id=1, source_target_pairs={{0,6},{2,0},{4,2},{6,4},{1,7},{3,1},{5,3},{7,5},{8,14},{10,8},{12,... | collective-permute-start | bytes 1880072 | tf_op jit(solution)/shard_map/ppermute | solution.py:31
  87.3 9.5 %collective-permute-done.7.refs_3_ = bf16[2448,128]{1,0:T(8,128)(2,1)S(1)} collective-permute-done((bf16[2448,128]{1,0:T(8,128)(2,1)S(1)}, bf16[2448,128]{1,0:T(8,128)(2,1)S(1)}, u32[]{:S(2)}, u32[]{:S(2)}) %collective-permute-start.7) | collective-permute-done | bytes 626720 | tf_op jit(solution)/shard_map/ppermute | solution.py:31
  98.2 17.2 %collective-permute-done.9.refs_5_ = bf16[2448,128]{1,0:T(8,128)(2,1)S(1)} collective-permute-done((bf16[2448,128]{1,0:T(8,128)(2,1)S(1)}, bf16[2448,128]{1,0:T(8,128)(2,1)S(1)}, u32[]{:S(2)}, u32[]{:S(2)}) %collective-permute-start.9) | collective-permute-done | bytes 626720 | tf_op jit(solution)/shard_map/ppermute | solution.py:31
  124.5 4.9 %shard_map.167 = (bf16[4,128,512]{2,1,0:T(8,128)(2,1)S(1)}, bf16[4,400,128]{2,1,0:T(8,128)(2,1)S(1)}) custom-call(s32[3]{0:T(128)S(1)} %pad_add_fusion.idx, bf16[16,128,256]{2,1,0:T(8,128)(2,1)S(1)} %copy-done.1, bf16[16,128,256]{2,1,0:T(8,128)(2,1)S(1)} %copy-done.9, bf16[2448,128]{1,0:T(8,128)(2,1)S(1)} %copy-done.7, bf16[2448,128]{1,0:T(8,128)(2,1)S(1)} %copy-done.11, ...), custom_call_target="tpu_custom_call" | custom-call | tf_op jit(solution)/shard_map/pallas_call | solution.py:53
  136.3 4.1 %all-to-all-start = ((bf16[4,128,512]{2,1,0:T(8,128)(2,1)}), bf16[4,128,512]{2,1,0:T(8,128)(2,1)}, u32[]{:S(2)}, u32[]{:S(2)}) async-start(bf16[4,128,512]{2,1,0:T(8,128)(2,1)} %copy-done.16), calls=%async_computation | async-start | bytes 1048576 | tf_op jit(solution)/shard_map/all_to_all | solution.py:465
  144.1 3.2 %collective-permute-start.25 = (bf16[2,128,1024]{2,1,0:T(8,128)(2,1)}, bf16[2,128,1024]{2,1,0:T(8,128)(2,1)}, u32[]{:S(2)}, u32[]{:S(2)}) collective-permute-start(bf16[2,128,1024]{2,1,0:T(8,128)(2,1)} %get-tuple-element.32), channel_id=1, source_target_pairs={{0,224},{32,0},{64,32},{96,64},{128,96},{160,128},{192,160},{224,1... | collective-permute-start | bytes 1572872 | tf_op jit(solution)/shard_map/ppermute | solution.py:31
  150.4 5.0 %shard_map.172 = (bf16[128,2048]{1,0:T(8,128)(2,1)S(1)}, bf16[128,2048]{1,0:T(8,128)(2,1)S(1)}) custom-call(s32[3]{0:T(128)S(1)} %copy-done.18, bf16[128,2048]{1,0:T(8,128)(2,1)} %refs_0_.7, f32[1,2048]{1,0:T(1,128)} %bitcast.15, bf16[4,128,512]{2,1,0:T(8,128)(2,1)} %all-to-all-done.refs_2_, bf16[4,400,128]{2,1,0:T(8,128)(2,1)S(1)} %get-tuple-element.27.refs_3_, ...), custom_call_target="tpu_custom_call" | custom-call | tf_op jit(solution)/shard_map/pallas_call | solution.py:53
  160.5 6.9 %collective-permute-done.34.refs_2_.near = bf16[128,2048]{1,0:T(8,128)(2,1)S(1)} collective-permute-done((bf16[128,2048]{1,0:T(8,128)(2,1)S(1)}, bf16[128,2048]{1,0:T(8,128)(2,1)S(1)}, u32[]{:S(2)}, u32[]{:S(2)}) %collective-permute-start.34) | collective-permute-done | bytes 524320 | tf_op jit(solution)/shard_map/ppermute | solution.py:31
  168.0 11.8 %collective-permute-done.35.refs_3_.back = bf16[128,2048]{1,0:T(8,128)(2,1)S(1)} collective-permute-done((bf16[128,2048]{1,0:T(8,128)(2,1)S(1)}, bf16[128,2048]{1,0:T(8,128)(2,1)S(1)}, u32[]{:S(2)}, u32[]{:S(2)}) %collective-permute-start.35) | collective-permute-done | bytes 524320 | tf_op jit(solution)/shard_map/ppermute | solution.py:31
  179.9 3.2 %collective-permute-start.37 = (bf16[64,2048]{1,0:T(8,128)(2,1)S(1)}, bf16[64,2048]{1,0:T(8,128)(2,1)S(1)}, u32[]{:S(2)}, u32[]{:S(2)}) collective-permute-start(bf16[64,2048]{1,0:T(8,128)(2,1)S(1)} %get-tuple-element.40), channel_id=1, source_target_pairs={{0,6},{2,0},{4,2},{6,4},{1,7},{3,1},{5,3},{7,5},{8,14},{10,8},{12,... | collective-permute-start | bytes 786440 | tf_op jit(solution)/shard_map/ppermute | solution.py:31
  183.2 3.3 %shard_map.180._ = bf16[2048,2048]{1,0:T(8,128)(2,1)S(1)} custom-call(s32[3]{0:T(128)S(1)} %copy-done.19, bf16[12,1024,128]{2,1,0:T(8,128)(2,1)} %shard_map.179.refs_0_, bf16[12,1024,128]{2,1,0:T(8,128)(2,1)} %collective-permute-done.33.refs_1_), custom_call_target="tpu_custom_call" | custom-call | tf_op jit(solution)/shard_map/pallas_call | solution.py:53
  190.3 3.7 %shard_map.185 = (bf16[64,2048]{1,0:T(8,128)(2,1)S(1)}, bf16[64,2048]{1,0:T(8,128)(2,1)S(1)}) custom-call(bf16[2048,2048]{1,0:T(8,128)(2,1)S(1)} %shard_map.176.refs_0_, bf16[2048,2048]{1,0:T(8,128)(2,1)S(1)} %shard_map.181.refs_1_, bf16[64,2048]{1,0:T(8,128)(2,1)S(1)} %collective-permute-done.36.refs_2_, bf16[64,2048]{1,0:T(8,128)(2,1)S(1)} %collective-permute-done.37.refs_3_), custom_call_target="tpu_custom_call" | custom-call | tf_op jit(solution)/shard_map/pallas_call | solution.py:53
  194.2 3.2 %collective-permute-start.39 = (bf16[64,2048]{1,0:T(8,128)(2,1)S(1)}, bf16[64,2048]{1,0:T(8,128)(2,1)S(1)}, u32[]{:S(2)}, u32[]{:S(2)}) collective-permute-start(bf16[64,2048]{1,0:T(8,128)(2,1)S(1)} %get-tuple-element.42), channel_id=1, source_target_pairs={{0,6},{2,0},{4,2},{6,4},{1,7},{3,1},{5,3},{7,5},{8,14},{10,8},{12,... | collective-permute-start | bytes 786440 | tf_op jit(solution)/shard_map/ppermute | solution.py:31
  197.4 5.8 %shard_map.183 = (bf16[128,2048]{1,0:T(8,128)(2,1)S(1)}, bf16[128,2048]{1,0:T(8,128)(2,1)S(1)}) custom-call(bf16[2048,2048]{1,0:T(8,128)(2,1)S(1)} %shard_map.176.refs_0_, bf16[2048,2048]{1,0:T(8,128)(2,1)S(1)} %shard_map.181.refs_1_, bf16[128,2048]{1,0:T(8,128)(2,1)S(1)} %collective-permute-done.34.refs_2_.near, ...), custom_call_target="tpu_custom_call" | custom-call | tf_op jit(solution)/shard_map/pallas_call | solution.py:53
  203.4 3.2 %collective-permute-start.41 = (bf16[128,2048]{1,0:T(8,128)(2,1)S(1)}, bf16[128,2048]{1,0:T(8,128)(2,1)S(1)}, u32[]{:S(2)}, u32[]{:S(2)}) collective-permute-start(bf16[128,2048]{1,0:T(8,128)(2,1)S(1)} %get-tuple-element.44), channel_id=1, source_target_pairs={{0,6},{2,0},{4,2},{6,4},{1,7},{3,1},{5,3},{7,5},{8,14},{10,8},{12,... | collective-permute-start | bytes 1572872 | tf_op jit(solution)/shard_map/ppermute | solution.py:31
  206.7 3.7 %shard_map.182 = bf16[128,2048]{1,0:T(8,128)(2,1)S(1)} custom-call(bf16[2048,2048]{1,0:T(8,128)(2,1)S(1)} %shard_map.176.refs_0_, bf16[2048,2048]{1,0:T(8,128)(2,1)S(1)} %shard_map.181.refs_1_, bf16[128,2048]{1,0:T(8,128)(2,1)S(1)} %get-tuple-element.36.refs_2_), custom_call_target="tpu_custom_call" | custom-call | tf_op jit(solution)/shard_map/pallas_call | solution.py:53
  210.4 3.4 %collective-permute-done.40 = bf16[128,2048]{1,0:T(8,128)(2,1)S(1)} collective-permute-done((bf16[128,2048]{1,0:T(8,128)(2,1)S(1)}, bf16[128,2048]{1,0:T(8,128)(2,1)S(1)}, u32[]{:S(2)}, u32[]{:S(2)}) %collective-permute-start.40) | collective-permute-done | bytes 524320 | tf_op jit(solution)/shard_map/ppermute | solution.py:31
  (128 shorter events, 75.7 us)
Async XLA Ops:
  3.5 15.2 %collective-permute-start.1 = (bf16[128,1280]{1,0:T(8,128)(2,1)S(1)}, bf16[128,1280]{1,0:T(8,128)(2,1)S(1)}, u32[]{:S(2)}, u32[]{:S(2)}) collective-permute-start(bf16[128,1280]{1,0:T(8,128)(2,1)S(1)} %shard_map.163.c0), channel_id=1, source_target_pairs={{0,16},{8,24},{16,0},{24,8},{1,17},{9,25},{17,1},{25,9},{2,18},{10... | collective-permute-start | bytes 983048 | tf_op jit(solution)/shard_map/ppermute | solution.py:31
  4.2 15.3 %collective-permute-start.2 = (bf16[128,1280]{1,0:T(8,128)(2,1)S(1)}, bf16[128,1280]{1,0:T(8,128)(2,1)S(1)}, u32[]{:S(2)}, u32[]{:S(2)}) collective-permute-start(bf16[128,1280]{1,0:T(8,128)(2,1)S(1)} %shard_map.163.c0), channel_id=1, source_target_pairs={{0,8},{8,16},{16,24},{24,0},{1,9},{9,17},{17,25},{25,1},{2,10},{10... | collective-permute-start | bytes 983048 | tf_op jit(solution)/shard_map/ppermute | solution.py:31
  7.2 18.4 %collective-permute-start.11 = (bf16[1152,128]{1,0:T(8,128)(2,1)S(1)}, bf16[1152,128]{1,0:T(8,128)(2,1)S(1)}, u32[]{:S(2)}, u32[]{:S(2)}) collective-permute-start(bf16[1152,128]{1,0:T(8,128)(2,1)S(1)} %shard_map.168.r0), channel_id=1, source_target_pairs={{0,224},{32,0},{64,32},{96,64},{128,96},{160,128},{192,160},{224,1... | collective-permute-start | bytes 884744 | tf_op jit(solution)/shard_map/ppermute | solution.py:31
  13.1 15.9 %collective-permute-start.13 = (bf16[1152,128]{1,0:T(8,128)(2,1)S(1)}, bf16[1152,128]{1,0:T(8,128)(2,1)S(1)}, u32[]{:S(2)}, u32[]{:S(2)}) collective-permute-start(bf16[1152,128]{1,0:T(8,128)(2,1)S(1)} %shard_map.168.r0), channel_id=1, source_target_pairs={{0,32},{32,64},{64,96},{96,128},{128,160},{160,192},{192,224},{224... | collective-permute-start | bytes 884744 | tf_op jit(solution)/shard_map/ppermute | solution.py:31
  19.7 27.6 %collective-permute-start.3 = (bf16[4,128,256]{2,1,0:T(8,128)(2,1)S(1)}, bf16[4,128,256]{2,1,0:T(8,128)(2,1)S(1)}, u32[]{:S(2)}, u32[]{:S(2)}) collective-permute-start(bf16[4,128,256]{2,1,0:T(8,128)(2,1)S(1)} %get-tuple-element.25.refs_0_), channel_id=1, source_target_pairs={{0,224},{32,0},{64,32},{96,64},{128,96},{160,128},{192,160},{224,1... | collective-permute-start | bytes 786440 | tf_op jit(solution)/shard_map/ppermute | solution.py:31
  40.6 23.3 %collective-permute-start.17 = (bf16[16,128,128]{2,1,0:T(8,128)(2,1)}, bf16[16,128,128]{2,1,0:T(8,128)(2,1)S(1)}, u32[]{:S(2)}, u32[]{:S(2)}) collective-permute-start(bf16[16,128,128]{2,1,0:T(8,128)(2,1)} %shard_map.170.refs_5_), channel_id=1, source_target_pairs={{0,6},{2,0},{4,2},{6,4},{1,7},{3,1},{5,3},{7,5},{8,14},{10,8},{12,... | collective-permute-start | bytes 1572872 | tf_op jit(solution)/shard_map/ppermute | solution.py:31
  43.7 38.7 %collective-permute-start.28 = (bf16[4,1024,128]{2,1,0:T(8,128)(2,1)S(1)}, bf16[4,1024,128]{2,1,0:T(8,128)(2,1)S(1)}, u32[]{:S(2)}, u32[]{:S(2)}) collective-permute-start(bf16[4,1024,128]{2,1,0:T(8,128)(2,1)S(1)} %get-tuple-element.33.refs_0_), channel_id=1, source_target_pairs={{0,24},{8,0},{16,8},{24,16},{1,25},{9,1},{17,9},{25,17},{2,26},{10... | collective-permute-start | bytes 3145736 | tf_op jit(solution)/shard_map/ppermute | solution.py:31
  46.6 17.3 %collective-permute-start.18 = (bf16[16,128,128]{2,1,0:T(8,128)(2,1)}, bf16[16,128,128]{2,1,0:T(8,128)(2,1)S(1)}, u32[]{:S(2)}, u32[]{:S(2)}) collective-permute-start(bf16[16,128,128]{2,1,0:T(8,128)(2,1)} %shard_map.170.refs_5_), channel_id=1, source_target_pairs={{0,4},{2,6},{4,0},{6,2},{1,5},{3,7},{5,1},{7,3},{8,12},{10,14},{12... | collective-permute-start | bytes 1572872 | tf_op jit(solution)/shard_map/ppermute | solution.py:31
  56.7 25.8 %collective-permute-start.29 = (bf16[4,1024,128]{2,1,0:T(8,128)(2,1)S(1)}, bf16[4,1024,128]{2,1,0:T(8,128)(2,1)S(1)}, u32[]{:S(2)}, u32[]{:S(2)}) collective-permute-start(bf16[4,1024,128]{2,1,0:T(8,128)(2,1)S(1)} %get-tuple-element.33.refs_0_), channel_id=1, source_target_pairs={{0,8},{8,16},{16,24},{24,0},{1,9},{9,17},{17,25},{25,1},{2,10},{10... | collective-permute-start | bytes 3145736 | tf_op jit(solution)/shard_map/ppermute | solution.py:31
  58.8 25.6 %collective-permute-start.22 = (bf16[4,128,1024]{2,1,0:T(8,128)(2,1)S(1)}, bf16[4,128,1024]{2,1,0:T(8,128)(2,1)S(1)}, u32[]{:S(2)}, u32[]{:S(2)}) collective-permute-start(bf16[4,128,1024]{2,1,0:T(8,128)(2,1)S(1)} %get-tuple-element.30.refs_0_), channel_id=1, source_target_pairs={{0,224},{32,0},{64,32},{96,64},{128,96},{160,128},{192,160},{224,1... | collective-permute-start | bytes 3145736 | tf_op jit(solution)/shard_map/ppermute | solution.py:31
  63.9 14.9 %collective-permute-start.19 = (bf16[16,128,128]{2,1,0:T(8,128)(2,1)}, bf16[16,128,128]{2,1,0:T(8,128)(2,1)S(1)}, u32[]{:S(2)}, u32[]{:S(2)}) collective-permute-start(bf16[16,128,128]{2,1,0:T(8,128)(2,1)} %shard_map.170.refs_5_), channel_id=1, source_target_pairs={{0,2},{2,4},{4,6},{6,0},{1,3},{3,5},{5,7},{7,1},{8,10},{10,12},{12... | collective-permute-start | bytes 1572872 | tf_op jit(solution)/shard_map/ppermute | solution.py:31
  63.9 22.4 %collective-permute-start.23 = (bf16[4,128,1024]{2,1,0:T(8,128)(2,1)S(1)}, bf16[4,128,1024]{2,1,0:T(8,128)(2,1)S(1)}, u32[]{:S(2)}, u32[]{:S(2)}) collective-permute-start(bf16[4,128,1024]{2,1,0:T(8,128)(2,1)S(1)} %get-tuple-element.30.refs_0_), channel_id=1, source_target_pairs={{0,32},{32,64},{64,96},{96,128},{128,160},{160,192},{192,224},{224... | collective-permute-start | bytes 3145736 | tf_op jit(solution)/shard_map/ppermute | solution.py:31
  78.9 18.0 %collective-permute-start.7 = (bf16[2448,128]{1,0:T(8,128)(2,1)S(1)}, bf16[2448,128]{1,0:T(8,128)(2,1)S(1)}, u32[]{:S(2)}, u32[]{:S(2)}) collective-permute-start(bf16[2448,128]{1,0:T(8,128)(2,1)S(1)} %shard_map.166.refs_2_), channel_id=1, source_target_pairs={{0,6},{2,0},{4,2},{6,4},{1,7},{3,1},{5,3},{7,5},{8,14},{10,8},{12,... | collective-permute-start | bytes 1880072 | tf_op jit(solution)/shard_map/ppermute | solution.py:31
  82.5 34.1 %collective-permute-start.6 = (bf16[16,128,256]{2,1,0:T(8,128)(2,1)S(1)}, bf16[16,128,256]{2,1,0:T(8,128)(2,1)S(1)}, u32[]{:S(2)}, u32[]{:S(2)}) collective-permute-start(bf16[16,128,256]{2,1,0:T(8,128)(2,1)S(1)} %shard_map.165.refs_0_), channel_id=1, source_target_pairs={{0,1},{1,0},{2,3},{3,2},{4,5},{5,4},{6,7},{7,6},{8,9},{9,8},{10,11... | collective-permute-start | bytes 3145736 | tf_op jit(solution)/shard_map/ppermute | solution.py:35
  84.5 95.5 %collective-permute-start.33 = (bf16[12,1024,128]{2,1,0:T(8,128)(2,1)}, bf16[12,1024,128]{2,1,0:T(8,128)(2,1)}, u32[]{:S(2)}, u32[]{:S(2)}) collective-permute-start(bf16[12,1024,128]{2,1,0:T(8,128)(2,1)} %shard_map.179.refs_0_), channel_id=1, source_target_pairs={{0,1},{1,0},{2,3},{3,2},{4,5},{5,4},{6,7},{7,6},{8,9},{9,8},{10,11... | collective-permute-start | bytes 9437192 | tf_op jit(solution)/shard_map/ppermute | solution.py:35
  86.3 57.7 %collective-permute-start.21 = (bf16[48,128,128]{2,1,0:T(8,128)(2,1)}, bf16[48,128,128]{2,1,0:T(8,128)(2,1)}, u32[]{:S(2)}, u32[]{:S(2)}) collective-permute-start(bf16[48,128,128]{2,1,0:T(8,128)(2,1)} %shard_map.171.refs_6_), channel_id=1, source_target_pairs={{0,1},{1,0},{2,3},{3,2},{4,5},{5,4},{6,7},{7,6},{8,9},{9,8},{10,11... | collective-permute-start | bytes 4718600 | tf_op jit(solution)/shard_map/ppermute | solution.py:35
  96.9 90.8 %collective-permute-start.26 = (bf16[12,128,1024]{2,1,0:T(8,128)(2,1)S(1)}, bf16[12,128,1024]{2,1,0:T(8,128)(2,1)}, u32[]{:S(2)}, u32[]{:S(2)}) collective-permute-start(bf16[12,128,1024]{2,1,0:T(8,128)(2,1)S(1)} %shard_map.173.refs_0_), channel_id=1, source_target_pairs={{0,1},{1,0},{2,3},{3,2},{4,5},{5,4},{6,7},{7,6},{8,9},{9,8},{10,11... | collective-permute-start | bytes 9437192 | tf_op jit(solution)/shard_map/ppermute | solution.py:35
  96.9 18.5 %collective-permute-start.9 = (bf16[2448,128]{1,0:T(8,128)(2,1)S(1)}, bf16[2448,128]{1,0:T(8,128)(2,1)S(1)}, u32[]{:S(2)}, u32[]{:S(2)}) collective-permute-start(bf16[2448,128]{1,0:T(8,128)(2,1)S(1)} %shard_map.166.refs_2_), channel_id=1, source_target_pairs={{0,2},{2,4},{4,6},{6,0},{1,3},{3,5},{5,7},{7,1},{8,10},{10,12},{12... | collective-permute-start | bytes 1880072 | tf_op jit(solution)/shard_map/ppermute | solution.py:31
  115.4 14.7 %collective-permute-start.20 = (bf16[16,128,128]{2,1,0:T(8,128)(2,1)}, bf16[16,128,128]{2,1,0:T(8,128)(2,1)}, u32[]{:S(2)}, u32[]{:S(2)}) collective-permute-start(bf16[16,128,128]{2,1,0:T(8,128)(2,1)} %shard_map.170.refs_5_), channel_id=1, source_target_pairs={{0,1},{1,0},{2,3},{3,2},{4,5},{5,4},{6,7},{7,6},{8,9},{9,8},{10,11... | collective-permute-start | bytes 1572872 | tf_op jit(solution)/shard_map/ppermute | solution.py:35
  117.6 15.8 %collective-permute-start.30 = (bf16[2,1024,128]{2,1,0:T(8,128)(2,1)}, bf16[2,1024,128]{2,1,0:T(8,128)(2,1)}, u32[]{:S(2)}, u32[]{:S(2)}) collective-permute-start(bf16[2,1024,128]{2,1,0:T(8,128)(2,1)} %get-tuple-element.34), channel_id=1, source_target_pairs={{0,8},{8,16},{16,24},{24,0},{1,9},{9,17},{17,25},{25,1},{2,10},{10... | collective-permute-start | bytes 1572872 | tf_op jit(solution)/shard_map/ppermute | solution.py:31
  133.4 22.0 %collective-permute-start.31 = (bf16[2,1024,128]{2,1,0:T(8,128)(2,1)}, bf16[2,1024,128]{2,1,0:T(8,128)(2,1)}, u32[]{:S(2)}, u32[]{:S(2)}) collective-permute-start(bf16[2,1024,128]{2,1,0:T(8,128)(2,1)} %get-tuple-element.35), channel_id=1, source_target_pairs={{0,24},{8,0},{16,8},{24,16},{1,25},{9,1},{17,9},{25,17},{2,26},{10... | collective-permute-start | bytes 1572872 | tf_op jit(solution)/shard_map/ppermute | solution.py:31
  144.0 14.7 %collective-permute-start.24 = (bf16[2,128,1024]{2,1,0:T(8,128)(2,1)}, bf16[2,128,1024]{2,1,0:T(8,128)(2,1)}, u32[]{:S(2)}, u32[]{:S(2)}) collective-permute-start(bf16[2,128,1024]{2,1,0:T(8,128)(2,1)} %get-tuple-element.31), channel_id=1, source_target_pairs={{0,32},{32,64},{64,96},{96,128},{128,160},{160,192},{192,224},{224... | collective-permute-start | bytes 1572872 | tf_op jit(solution)/shard_map/ppermute | solution.py:31
  158.7 27.8 %collective-permute-start.32 = (bf16[4,1024,128]{2,1,0:T(8,128)(2,1)S(1)}, bf16[4,1024,128]{2,1,0:T(8,128)(2,1)S(1)}, u32[]{:S(2)}, u32[]{:S(2)}) collective-permute-start(bf16[4,1024,128]{2,1,0:T(8,128)(2,1)S(1)} %shard_map.178.own), channel_id=1, source_target_pairs={{0,1},{1,0},{2,3},{3,2},{4,5},{5,4},{6,7},{7,6},{8,9},{9,8},{10,11... | collective-permute-start | bytes 3145736 | tf_op jit(solution)/shard_map/ppermute | solution.py:35
  160.0 27.7 %collective-permute-start.27 = (bf16[4,128,1024]{2,1,0:T(8,128)(2,1)S(1)}, bf16[4,128,1024]{2,1,0:T(8,128)(2,1)S(1)}, u32[]{:S(2)}, u32[]{:S(2)}) collective-permute-start(bf16[4,128,1024]{2,1,0:T(8,128)(2,1)S(1)} %shard_map.175.refs_1_), channel_id=1, source_target_pairs={{0,1},{1,0},{2,3},{3,2},{4,5},{5,4},{6,7},{7,6},{8,9},{9,8},{10,11... | collective-permute-start | bytes 3145736 | tf_op jit(solution)/shard_map/ppermute | solution.py:35
  (39 other events, 334.5 us)

commit v3 on v2

--- a/solution.py
+++ b/solution.py
@@ -169,9 +169,12 @@
     finish(copies([(back.at[:2], low), (near.at[2:], high)], sem))
 
 
-def row_halves_kernel(near, back, low, high):
-    low[...] = back[:HALF]
-    high[...] = near[HALF:]
+def low_kernel(rows, out):
+    out[...] = rows[:HALF]
+
+
+def high_kernel(rows, out):
+    out[...] = rows[HALF:]
 
 
 def joined(arrays):
@@ -493,7 +496,8 @@
         16,
     )
     near_rows, back_rows = shift(normed, "y", -1), shift(normed, "y", 1)
-    low, high = call(row_halves_kernel, [((HALF, D), BF)] * 2, (near_rows, back_rows), [VM] * 2, [])
+    (high,) = call(high_kernel, [((HALF, D), BF)], (near_rows,), [VM], [])
+    (low,) = call(low_kernel, [((HALF, D), BF)], (back_rows,), [VM], [])
     far_rows = shift(low, "y", 1), shift(high, "y", -1)
     dma = [pltpu.SemaphoreType.DMA(())]
     (up,) = call(up_kernel, [((D, 2 * FF_DEV), BF)], (idx, *expands), [SM] + [HB] * 4, dma)

time: 219 us -> 219 us (level)
    pallas_call x24 -> x25, Pallas kernels: 43.7 us -> 43.6 us  [call(): pl.pallas_call(kernel, out_shape=[jax.ShapeDtypeStruct(s, d) for s, d in...]
where the time goes in v3:
time: 219 us; the launch traced here: 216 us
  waiting for transfers between devices  93.6 us (43%)
  starting transfers between devices  64.6 us (29%)
  Pallas kernels  43.6 us (20%)
  local copies, waits for them, and re-layouts  12.2 us (6%)
    ppermute x34, waiting for transfers between devices, shift(): return lax.ppermute(x, axis, pairs)  91.2 us
    ppermute x34, starting transfers between devices, shift(): return lax.ppermute(x, axis, pairs)  58.5 us
    pallas_call x25, Pallas kernels, call(): pl.pallas_call(kernel, out_shape=[jax.ShapeDtypeStruct(s, d) for s, d in...  43.6 us
    unnamed x40, local copies, waits for them, and re-layouts  12.2 us
  transfers between devices with their start and end apart: 43, of which 17 were waited for; matrix products, arithmetic and copies ran while one was open for 0% of the time, Pallas kernels for 18%

profile of v3, /device:TPU:2, one launch (start us, length us, event | category | flops | bytes accessed | tf_op | source)
XLA Modules:
  0.0 215.8 jit_solution(5178772454373397232)
XLA Ops:
  7.2 5.9 %collective-permute-start.11 = (bf16[1152,128]{1,0:T(8,128)(2,1)S(1)}, bf16[1152,128]{1,0:T(8,128)(2,1)S(1)}, u32[]{:S(2)}, u32[]{:S(2)}) collective-permute-start(bf16[1152,128]{1,0:T(8,128)(2,1)S(1)} %shard_map.168.r0), channel_id=1, source_target_pairs={{0,224},{32,0},{64,32},{96,64},{128,96},{160,128},{192,160},{224,1... | collective-permute-start | bytes 884744 | tf_op jit(solution)/shard_map/ppermute | solution.py:31
  19.7 5.9 %collective-permute-start.3 = (bf16[4,128,256]{2,1,0:T(8,128)(2,1)S(1)}, bf16[4,128,256]{2,1,0:T(8,128)(2,1)S(1)}, u32[]{:S(2)}, u32[]{:S(2)}) collective-permute-start(bf16[4,128,256]{2,1,0:T(8,128)(2,1)S(1)} %get-tuple-element.23.refs_0_), channel_id=1, source_target_pairs={{0,224},{32,0},{64,32},{96,64},{128,96},{160,128},{192,160},{224,1... | collective-permute-start | bytes 786440 | tf_op jit(solution)/shard_map/ppermute | solution.py:31
  25.6 3.4 %collective-permute-done.13.r3 = bf16[1152,128]{1,0:T(8,128)(2,1)S(1)} collective-permute-done((bf16[1152,128]{1,0:T(8,128)(2,1)S(1)}, bf16[1152,128]{1,0:T(8,128)(2,1)S(1)}, u32[]{:S(2)}, u32[]{:S(2)}) %collective-permute-start.13) | collective-permute-done | bytes 294944 | tf_op jit(solution)/shard_map/ppermute | solution.py:31
  29.6 3.8 %collective-permute-start.15 = (bf16[4,128,128]{2,1,0:T(8,128)(2,1)S(1)}, bf16[4,128,128]{2,1,0:T(8,128)(2,1)S(1)}, u32[]{:S(2)}, u32[]{:S(2)}) collective-permute-start(bf16[4,128,128]{2,1,0:T(8,128)(2,1)S(1)} %get-tuple-element.26.refs_0_), channel_id=1, source_target_pairs={{0,16},{8,24},{16,0},{24,8},{1,17},{9,25},{17,1},{25,9},{2,18},{10... | collective-permute-start | bytes 393224 | tf_op jit(solution)/shard_map/ppermute | solution.py:31
  50.4 6.3 %collective-permute-done.4.refs_2_ = bf16[4,128,256]{2,1,0:T(8,128)(2,1)S(1)} collective-permute-done((bf16[4,128,256]{2,1,0:T(8,128)(2,1)S(1)}, bf16[4,128,256]{2,1,0:T(8,128)(2,1)S(1)}, u32[]{:S(2)}, u32[]{:S(2)}) %collective-permute-start.4) | collective-permute-done | bytes 262176 | tf_op jit(solution)/shard_map/ppermute | solution.py:31
  60.0 3.9 %collective-permute-done.17.refs_0_ = bf16[16,128,128]{2,1,0:T(8,128)(2,1)S(1)} collective-permute-done((bf16[16,128,128]{2,1,0:T(8,128)(2,1)}, bf16[16,128,128]{2,1,0:T(8,128)(2,1)S(1)}, u32[]{:S(2)}, u32[]{:S(2)}) %collective-permute-start.17) | collective-permute-done | bytes 524320 | tf_op jit(solution)/shard_map/ppermute | solution.py:31
  65.3 13.6 %collective-permute-done.19.refs_2_ = bf16[16,128,128]{2,1,0:T(8,128)(2,1)S(1)} collective-permute-done((bf16[16,128,128]{2,1,0:T(8,128)(2,1)}, bf16[16,128,128]{2,1,0:T(8,128)(2,1)S(1)}, u32[]{:S(2)}, u32[]{:S(2)}) %collective-permute-start.19) | collective-permute-done | bytes 524320 | tf_op jit(solution)/shard_map/ppermute | solution.py:31
  78.9 3.5 %collective-permute-start.7 = (bf16[2448,128]{1,0:T(8,128)(2,1)S(1)}, bf16[2448,128]{1,0:T(8,128)(2,1)S(1)}, u32[]{:S(2)}, u32[]{:S(2)}) collective-permute-start(bf16[2448,128]{1,0:T(8,128)(2,1)S(1)} %shard_map.166.refs_2_), channel_id=1, source_target_pairs={{0,6},{2,0},{4,2},{6,4},{1,7},{3,1},{5,3},{7,5},{8,14},{10,8},{12,... | collective-permute-start | bytes 1880072 | tf_op jit(solution)/shard_map/ppermute | solution.py:31
  87.3 9.5 %collective-permute-done.7.refs_3_ = bf16[2448,128]{1,0:T(8,128)(2,1)S(1)} collective-permute-done((bf16[2448,128]{1,0:T(8,128)(2,1)S(1)}, bf16[2448,128]{1,0:T(8,128)(2,1)S(1)}, u32[]{:S(2)}, u32[]{:S(2)}) %collective-permute-start.7) | collective-permute-done | bytes 626720 | tf_op jit(solution)/shard_map/ppermute | solution.py:31
  98.2 17.2 %collective-permute-done.9.refs_5_ = bf16[2448,128]{1,0:T(8,128)(2,1)S(1)} collective-permute-done((bf16[2448,128]{1,0:T(8,128)(2,1)S(1)}, bf16[2448,128]{1,0:T(8,128)(2,1)S(1)}, u32[]{:S(2)}, u32[]{:S(2)}) %collective-permute-start.9) | collective-permute-done | bytes 626720 | tf_op jit(solution)/shard_map/ppermute | solution.py:31
  124.4 4.9 %shard_map.167 = (bf16[4,128,512]{2,1,0:T(8,128)(2,1)S(1)}, bf16[4,400,128]{2,1,0:T(8,128)(2,1)S(1)}) custom-call(s32[3]{0:T(128)S(1)} %pad_add_fusion.idx, bf16[16,128,256]{2,1,0:T(8,128)(2,1)S(1)} %copy-done.1, bf16[16,128,256]{2,1,0:T(8,128)(2,1)S(1)} %copy-done.9, bf16[2448,128]{1,0:T(8,128)(2,1)S(1)} %copy-done.7, bf16[2448,128]{1,0:T(8,128)(2,1)S(1)} %copy-done.11, ...), custom_call_target="tpu_custom_call" | custom-call | tf_op jit(solution)/shard_map/pallas_call | solution.py:53
  136.3 4.1 %all-to-all-start = ((bf16[4,128,512]{2,1,0:T(8,128)(2,1)}), bf16[4,128,512]{2,1,0:T(8,128)(2,1)}, u32[]{:S(2)}, u32[]{:S(2)}) async-start(bf16[4,128,512]{2,1,0:T(8,128)(2,1)} %copy-done.16), calls=%async_computation | async-start | bytes 1048576 | tf_op jit(solution)/shard_map/all_to_all | solution.py:468
  144.1 3.2 %collective-permute-start.25 = (bf16[2,128,1024]{2,1,0:T(8,128)(2,1)}, bf16[2,128,1024]{2,1,0:T(8,128)(2,1)}, u32[]{:S(2)}, u32[]{:S(2)}) collective-permute-start(bf16[2,128,1024]{2,1,0:T(8,128)(2,1)} %get-tuple-element.30), channel_id=1, source_target_pairs={{0,224},{32,0},{64,32},{96,64},{128,96},{160,128},{192,160},{224,1... | collective-permute-start | bytes 1572872 | tf_op jit(solution)/shard_map/ppermute | solution.py:31
  150.4 5.0 %shard_map.172 = (bf16[128,2048]{1,0:T(8,128)(2,1)S(1)}, bf16[128,2048]{1,0:T(8,128)(2,1)S(1)}) custom-call(s32[3]{0:T(128)S(1)} %copy-done.18, bf16[128,2048]{1,0:T(8,128)(2,1)} %refs_0_.7, f32[1,2048]{1,0:T(1,128)} %bitcast.15, bf16[4,128,512]{2,1,0:T(8,128)(2,1)} %all-to-all-done.refs_2_, bf16[4,400,128]{2,1,0:T(8,128)(2,1)S(1)} %get-tuple-element.25.refs_3_, ...), custom_call_target="tpu_custom_call" | custom-call | tf_op jit(solution)/shard_map/pallas_call | solution.py:53
  160.5 8.1 %collective-permute-done.35.refs_3_.rows = bf16[128,2048]{1,0:T(8,128)(2,1)S(1)} collective-permute-done((bf16[128,2048]{1,0:T(8,128)(2,1)S(1)}, bf16[128,2048]{1,0:T(8,128)(2,1)S(1)}, u32[]{:S(2)}, u32[]{:S(2)}) %collective-permute-start.35) | collective-permute-done | bytes 524320 | tf_op jit(solution)/shard_map/ppermute | solution.py:31
  168.7 11.9 %collective-permute-done.34.refs_2_.rows = bf16[128,2048]{1,0:T(8,128)(2,1)S(1)} collective-permute-done((bf16[128,2048]{1,0:T(8,128)(2,1)S(1)}, bf16[128,2048]{1,0:T(8,128)(2,1)S(1)}, u32[]{:S(2)}, u32[]{:S(2)}) %collective-permute-start.34) | collective-permute-done | bytes 524320 | tf_op jit(solution)/shard_map/ppermute | solution.py:31
  180.7 3.3 %collective-permute-start.37 = (bf16[64,2048]{1,0:T(8,128)(2,1)S(1)}, bf16[64,2048]{1,0:T(8,128)(2,1)S(1)}, u32[]{:S(2)}, u32[]{:S(2)}) collective-permute-start(bf16[64,2048]{1,0:T(8,128)(2,1)S(1)} %shard_map.185), channel_id=1, source_target_pairs={{0,6},{2,0},{4,2},{6,4},{1,7},{3,1},{5,3},{7,5},{8,14},{10,8},{12,... | collective-permute-start | bytes 786440 | tf_op jit(solution)/shard_map/ppermute | solution.py:31
  184.0 3.3 %shard_map.180._ = bf16[2048,2048]{1,0:T(8,128)(2,1)S(1)} custom-call(s32[3]{0:T(128)S(1)} %copy-done.19, bf16[12,1024,128]{2,1,0:T(8,128)(2,1)} %shard_map.179.refs_0_, bf16[12,1024,128]{2,1,0:T(8,128)(2,1)} %collective-permute-done.33.refs_1_), custom_call_target="tpu_custom_call" | custom-call | tf_op jit(solution)/shard_map/pallas_call | solution.py:53
  191.2 3.7 %shard_map.186 = (bf16[64,2048]{1,0:T(8,128)(2,1)S(1)}, bf16[64,2048]{1,0:T(8,128)(2,1)S(1)}) custom-call(bf16[2048,2048]{1,0:T(8,128)(2,1)S(1)} %shard_map.176.refs_0_, bf16[2048,2048]{1,0:T(8,128)(2,1)S(1)} %shard_map.181.refs_1_, bf16[64,2048]{1,0:T(8,128)(2,1)S(1)} %collective-permute-done.36.refs_2_, bf16[64,2048]{1,0:T(8,128)(2,1)S(1)} %collective-permute-done.37.refs_3_), custom_call_target="tpu_custom_call" | custom-call | tf_op jit(solution)/shard_map/pallas_call | solution.py:53
  195.0 3.2 %collective-permute-start.39 = (bf16[64,2048]{1,0:T(8,128)(2,1)S(1)}, bf16[64,2048]{1,0:T(8,128)(2,1)S(1)}, u32[]{:S(2)}, u32[]{:S(2)}) collective-permute-start(bf16[64,2048]{1,0:T(8,128)(2,1)S(1)} %get-tuple-element.38), channel_id=1, source_target_pairs={{0,6},{2,0},{4,2},{6,4},{1,7},{3,1},{5,3},{7,5},{8,14},{10,8},{12,... | collective-permute-start | bytes 786440 | tf_op jit(solution)/shard_map/ppermute | solution.py:31
  198.2 5.8 %shard_map.183 = (bf16[128,2048]{1,0:T(8,128)(2,1)S(1)}, bf16[128,2048]{1,0:T(8,128)(2,1)S(1)}) custom-call(bf16[2048,2048]{1,0:T(8,128)(2,1)S(1)} %shard_map.176.refs_0_, bf16[2048,2048]{1,0:T(8,128)(2,1)S(1)} %shard_map.181.refs_1_, bf16[128,2048]{1,0:T(8,128)(2,1)S(1)} %collective-permute-done.34.refs_2_.rows, ...), custom_call_target="tpu_custom_call" | custom-call | tf_op jit(solution)/shard_map/pallas_call | solution.py:53
  204.3 3.2 %collective-permute-start.41 = (bf16[128,2048]{1,0:T(8,128)(2,1)S(1)}, bf16[128,2048]{1,0:T(8,128)(2,1)S(1)}, u32[]{:S(2)}, u32[]{:S(2)}) collective-permute-start(bf16[128,2048]{1,0:T(8,128)(2,1)S(1)} %get-tuple-element.40), channel_id=1, source_target_pairs={{0,6},{2,0},{4,2},{6,4},{1,7},{3,1},{5,3},{7,5},{8,14},{10,8},{12,... | collective-permute-start | bytes 1572872 | tf_op jit(solution)/shard_map/ppermute | solution.py:31
  207.5 3.7 %shard_map.182 = bf16[128,2048]{1,0:T(8,128)(2,1)S(1)} custom-call(bf16[2048,2048]{1,0:T(8,128)(2,1)S(1)} %shard_map.176.refs_0_, bf16[2048,2048]{1,0:T(8,128)(2,1)S(1)} %shard_map.181.refs_1_, bf16[128,2048]{1,0:T(8,128)(2,1)S(1)} %get-tuple-element.34.refs_2_), custom_call_target="tpu_custom_call" | custom-call | tf_op jit(solution)/shard_map/pallas_call | solution.py:53
  211.3 3.4 %collective-permute-done.40 = bf16[128,2048]{1,0:T(8,128)(2,1)S(1)} collective-permute-done((bf16[128,2048]{1,0:T(8,128)(2,1)S(1)}, bf16[128,2048]{1,0:T(8,128)(2,1)S(1)}, u32[]{:S(2)}, u32[]{:S(2)}) %collective-permute-start.40) | collective-permute-done | bytes 524320 | tf_op jit(solution)/shard_map/ppermute | solution.py:31
  (129 shorter events, 75.1 us)
Async XLA Ops:
  3.5 15.2 %collective-permute-start.1 = (bf16[128,1280]{1,0:T(8,128)(2,1)S(1)}, bf16[128,1280]{1,0:T(8,128)(2,1)S(1)}, u32[]{:S(2)}, u32[]{:S(2)}) collective-permute-start(bf16[128,1280]{1,0:T(8,128)(2,1)S(1)} %shard_map.163.c0), channel_id=1, source_target_pairs={{0,16},{8,24},{16,0},{24,8},{1,17},{9,25},{17,1},{25,9},{2,18},{10... | collective-permute-start | bytes 983048 | tf_op jit(solution)/shard_map/ppermute | solution.py:31
  4.2 15.3 %collective-permute-start.2 = (bf16[128,1280]{1,0:T(8,128)(2,1)S(1)}, bf16[128,1280]{1,0:T(8,128)(2,1)S(1)}, u32[]{:S(2)}, u32[]{:S(2)}) collective-permute-start(bf16[128,1280]{1,0:T(8,128)(2,1)S(1)} %shard_map.163.c0), channel_id=1, source_target_pairs={{0,8},{8,16},{16,24},{24,0},{1,9},{9,17},{17,25},{25,1},{2,10},{10... | collective-permute-start | bytes 983048 | tf_op jit(solution)/shard_map/ppermute | solution.py:31
  7.2 18.4 %collective-permute-start.11 = (bf16[1152,128]{1,0:T(8,128)(2,1)S(1)}, bf16[1152,128]{1,0:T(8,128)(2,1)S(1)}, u32[]{:S(2)}, u32[]{:S(2)}) collective-permute-start(bf16[1152,128]{1,0:T(8,128)(2,1)S(1)} %shard_map.168.r0), channel_id=1, source_target_pairs={{0,224},{32,0},{64,32},{96,64},{128,96},{160,128},{192,160},{224,1... | collective-permute-start | bytes 884744 | tf_op jit(solution)/shard_map/ppermute | solution.py:31
  13.1 15.9 %collective-permute-start.13 = (bf16[1152,128]{1,0:T(8,128)(2,1)S(1)}, bf16[1152,128]{1,0:T(8,128)(2,1)S(1)}, u32[]{:S(2)}, u32[]{:S(2)}) collective-permute-start(bf16[1152,128]{1,0:T(8,128)(2,1)S(1)} %shard_map.168.r0), channel_id=1, source_target_pairs={{0,32},{32,64},{64,96},{96,128},{128,160},{160,192},{192,224},{224... | collective-permute-start | bytes 884744 | tf_op jit(solution)/shard_map/ppermute | solution.py:31
  19.7 27.6 %collective-permute-start.3 = (bf16[4,128,256]{2,1,0:T(8,128)(2,1)S(1)}, bf16[4,128,256]{2,1,0:T(8,128)(2,1)S(1)}, u32[]{:S(2)}, u32[]{:S(2)}) collective-permute-start(bf16[4,128,256]{2,1,0:T(8,128)(2,1)S(1)} %get-tuple-element.23.refs_0_), channel_id=1, source_target_pairs={{0,224},{32,0},{64,32},{96,64},{128,96},{160,128},{192,160},{224,1... | collective-permute-start | bytes 786440 | tf_op jit(solution)/shard_map/ppermute | solution.py:31
  40.6 23.3 %collective-permute-start.17 = (bf16[16,128,128]{2,1,0:T(8,128)(2,1)}, bf16[16,128,128]{2,1,0:T(8,128)(2,1)S(1)}, u32[]{:S(2)}, u32[]{:S(2)}) collective-permute-start(bf16[16,128,128]{2,1,0:T(8,128)(2,1)} %shard_map.170.refs_5_), channel_id=1, source_target_pairs={{0,6},{2,0},{4,2},{6,4},{1,7},{3,1},{5,3},{7,5},{8,14},{10,8},{12,... | collective-permute-start | bytes 1572872 | tf_op jit(solution)/shard_map/ppermute | solution.py:31
  43.7 38.7 %collective-permute-start.28 = (bf16[4,1024,128]{2,1,0:T(8,128)(2,1)S(1)}, bf16[4,1024,128]{2,1,0:T(8,128)(2,1)S(1)}, u32[]{:S(2)}, u32[]{:S(2)}) collective-permute-start(bf16[4,1024,128]{2,1,0:T(8,128)(2,1)S(1)} %get-tuple-element.31.refs_0_), channel_id=1, source_target_pairs={{0,24},{8,0},{16,8},{24,16},{1,25},{9,1},{17,9},{25,17},{2,26},{10... | collective-permute-start | bytes 3145736 | tf_op jit(solution)/shard_map/ppermute | solution.py:31
  46.6 17.3 %collective-permute-start.18 = (bf16[16,128,128]{2,1,0:T(8,128)(2,1)}, bf16[16,128,128]{2,1,0:T(8,128)(2,1)S(1)}, u32[]{:S(2)}, u32[]{:S(2)}) collective-permute-start(bf16[16,128,128]{2,1,0:T(8,128)(2,1)} %shard_map.170.refs_5_), channel_id=1, source_target_pairs={{0,4},{2,6},{4,0},{6,2},{1,5},{3,7},{5,1},{7,3},{8,12},{10,14},{12... | collective-permute-start | bytes 1572872 | tf_op jit(solution)/shard_map/ppermute | solution.py:31
  56.7 25.8 %collective-permute-start.29 = (bf16[4,1024,128]{2,1,0:T(8,128)(2,1)S(1)}, bf16[4,1024,128]{2,1,0:T(8,128)(2,1)S(1)}, u32[]{:S(2)}, u32[]{:S(2)}) collective-permute-start(bf16[4,1024,128]{2,1,0:T(8,128)(2,1)S(1)} %get-tuple-element.31.refs_0_), channel_id=1, source_target_pairs={{0,8},{8,16},{16,24},{24,0},{1,9},{9,17},{17,25},{25,1},{2,10},{10... | collective-permute-start | bytes 3145736 | tf_op jit(solution)/shard_map/ppermute | solution.py:31
  58.8 25.6 %collective-permute-start.22 = (bf16[4,128,1024]{2,1,0:T(8,128)(2,1)S(1)}, bf16[4,128,1024]{2,1,0:T(8,128)(2,1)S(1)}, u32[]{:S(2)}, u32[]{:S(2)}) collective-permute-start(bf16[4,128,1024]{2,1,0:T(8,128)(2,1)S(1)} %get-tuple-element.28.refs_0_), channel_id=1, source_target_pairs={{0,224},{32,0},{64,32},{96,64},{128,96},{160,128},{192,160},{224,1... | collective-permute-start | bytes 3145736 | tf_op jit(solution)/shard_map/ppermute | solution.py:31
  63.9 14.9 %collective-permute-start.19 = (bf16[16,128,128]{2,1,0:T(8,128)(2,1)}, bf16[16,128,128]{2,1,0:T(8,128)(2,1)S(1)}, u32[]{:S(2)}, u32[]{:S(2)}) collective-permute-start(bf16[16,128,128]{2,1,0:T(8,128)(2,1)} %shard_map.170.refs_5_), channel_id=1, source_target_pairs={{0,2},{2,4},{4,6},{6,0},{1,3},{3,5},{5,7},{7,1},{8,10},{10,12},{12... | collective-permute-start | bytes 1572872 | tf_op jit(solution)/shard_map/ppermute | solution.py:31
  63.9 22.4 %collective-permute-start.23 = (bf16[4,128,1024]{2,1,0:T(8,128)(2,1)S(1)}, bf16[4,128,1024]{2,1,0:T(8,128)(2,1)S(1)}, u32[]{:S(2)}, u32[]{:S(2)}) collective-permute-start(bf16[4,128,1024]{2,1,0:T(8,128)(2,1)S(1)} %get-tuple-element.28.refs_0_), channel_id=1, source_target_pairs={{0,32},{32,64},{64,96},{96,128},{128,160},{160,192},{192,224},{224... | collective-permute-start | bytes 3145736 | tf_op jit(solution)/shard_map/ppermute | solution.py:31
  78.9 18.0 %collective-permute-start.7 = (bf16[2448,128]{1,0:T(8,128)(2,1)S(1)}, bf16[2448,128]{1,0:T(8,128)(2,1)S(1)}, u32[]{:S(2)}, u32[]{:S(2)}) collective-permute-start(bf16[2448,128]{1,0:T(8,128)(2,1)S(1)} %shard_map.166.refs_2_), channel_id=1, source_target_pairs={{0,6},{2,0},{4,2},{6,4},{1,7},{3,1},{5,3},{7,5},{8,14},{10,8},{12,... | collective-permute-start | bytes 1880072 | tf_op jit(solution)/shard_map/ppermute | solution.py:31
  82.5 34.1 %collective-permute-start.6 = (bf16[16,128,256]{2,1,0:T(8,128)(2,1)S(1)}, bf16[16,128,256]{2,1,0:T(8,128)(2,1)S(1)}, u32[]{:S(2)}, u32[]{:S(2)}) collective-permute-start(bf16[16,128,256]{2,1,0:T(8,128)(2,1)S(1)} %shard_map.165.refs_0_), channel_id=1, source_target_pairs={{0,1},{1,0},{2,3},{3,2},{4,5},{5,4},{6,7},{7,6},{8,9},{9,8},{10,11... | collective-permute-start | bytes 3145736 | tf_op jit(solution)/shard_map/ppermute | solution.py:35
  84.4 96.2 %collective-permute-start.33 = (bf16[12,1024,128]{2,1,0:T(8,128)(2,1)}, bf16[12,1024,128]{2,1,0:T(8,128)(2,1)}, u32[]{:S(2)}, u32[]{:S(2)}) collective-permute-start(bf16[12,1024,128]{2,1,0:T(8,128)(2,1)} %shard_map.179.refs_0_), channel_id=1, source_target_pairs={{0,1},{1,0},{2,3},{3,2},{4,5},{5,4},{6,7},{7,6},{8,9},{9,8},{10,11... | collective-permute-start | bytes 9437192 | tf_op jit(solution)/shard_map/ppermute | solution.py:35
  86.3 57.7 %collective-permute-start.21 = (bf16[48,128,128]{2,1,0:T(8,128)(2,1)}, bf16[48,128,128]{2,1,0:T(8,128)(2,1)}, u32[]{:S(2)}, u32[]{:S(2)}) collective-permute-start(bf16[48,128,128]{2,1,0:T(8,128)(2,1)} %shard_map.171.refs_6_), channel_id=1, source_target_pairs={{0,1},{1,0},{2,3},{3,2},{4,5},{5,4},{6,7},{7,6},{8,9},{9,8},{10,11... | collective-permute-start | bytes 4718600 | tf_op jit(solution)/shard_map/ppermute | solution.py:35
  96.9 91.7 %collective-permute-start.26 = (bf16[12,128,1024]{2,1,0:T(8,128)(2,1)S(1)}, bf16[12,128,1024]{2,1,0:T(8,128)(2,1)}, u32[]{:S(2)}, u32[]{:S(2)}) collective-permute-start(bf16[12,128,1024]{2,1,0:T(8,128)(2,1)S(1)} %shard_map.173.refs_0_), channel_id=1, source_target_pairs={{0,1},{1,0},{2,3},{3,2},{4,5},{5,4},{6,7},{7,6},{8,9},{9,8},{10,11... | collective-permute-start | bytes 9437192 | tf_op jit(solution)/shard_map/ppermute | solution.py:35
  96.9 18.5 %collective-permute-start.9 = (bf16[2448,128]{1,0:T(8,128)(2,1)S(1)}, bf16[2448,128]{1,0:T(8,128)(2,1)S(1)}, u32[]{:S(2)}, u32[]{:S(2)}) collective-permute-start(bf16[2448,128]{1,0:T(8,128)(2,1)S(1)} %shard_map.166.refs_2_), channel_id=1, source_target_pairs={{0,2},{2,4},{4,6},{6,0},{1,3},{3,5},{5,7},{7,1},{8,10},{10,12},{12... | collective-permute-start | bytes 1880072 | tf_op jit(solution)/shard_map/ppermute | solution.py:31
  115.4 14.7 %collective-permute-start.20 = (bf16[16,128,128]{2,1,0:T(8,128)(2,1)}, bf16[16,128,128]{2,1,0:T(8,128)(2,1)}, u32[]{:S(2)}, u32[]{:S(2)}) collective-permute-start(bf16[16,128,128]{2,1,0:T(8,128)(2,1)} %shard_map.170.refs_5_), channel_id=1, source_target_pairs={{0,1},{1,0},{2,3},{3,2},{4,5},{5,4},{6,7},{7,6},{8,9},{9,8},{10,11... | collective-permute-start | bytes 1572872 | tf_op jit(solution)/shard_map/ppermute | solution.py:35
  117.6 15.8 %collective-permute-start.30 = (bf16[2,1024,128]{2,1,0:T(8,128)(2,1)}, bf16[2,1024,128]{2,1,0:T(8,128)(2,1)}, u32[]{:S(2)}, u32[]{:S(2)}) collective-permute-start(bf16[2,1024,128]{2,1,0:T(8,128)(2,1)} %get-tuple-element.32), channel_id=1, source_target_pairs={{0,8},{8,16},{16,24},{24,0},{1,9},{9,17},{17,25},{25,1},{2,10},{10... | collective-permute-start | bytes 1572872 | tf_op jit(solution)/shard_map/ppermute | solution.py:31
  133.3 22.0 %collective-permute-start.31 = (bf16[2,1024,128]{2,1,0:T(8,128)(2,1)}, bf16[2,1024,128]{2,1,0:T(8,128)(2,1)}, u32[]{:S(2)}, u32[]{:S(2)}) collective-permute-start(bf16[2,1024,128]{2,1,0:T(8,128)(2,1)} %get-tuple-element.33), channel_id=1, source_target_pairs={{0,24},{8,0},{16,8},{24,16},{1,25},{9,1},{17,9},{25,17},{2,26},{10... | collective-permute-start | bytes 1572872 | tf_op jit(solution)/shard_map/ppermute | solution.py:31
  144.0 14.7 %collective-permute-start.24 = (bf16[2,128,1024]{2,1,0:T(8,128)(2,1)}, bf16[2,128,1024]{2,1,0:T(8,128)(2,1)}, u32[]{:S(2)}, u32[]{:S(2)}) collective-permute-start(bf16[2,128,1024]{2,1,0:T(8,128)(2,1)} %get-tuple-element.29), channel_id=1, source_target_pairs={{0,32},{32,64},{64,96},{96,128},{128,160},{160,192},{192,224},{224... | collective-permute-start | bytes 1572872 | tf_op jit(solution)/shard_map/ppermute | solution.py:31
  158.7 28.6 %collective-permute-start.32 = (bf16[4,1024,128]{2,1,0:T(8,128)(2,1)S(1)}, bf16[4,1024,128]{2,1,0:T(8,128)(2,1)S(1)}, u32[]{:S(2)}, u32[]{:S(2)}) collective-permute-start(bf16[4,1024,128]{2,1,0:T(8,128)(2,1)S(1)} %shard_map.178.own), channel_id=1, source_target_pairs={{0,1},{1,0},{2,3},{3,2},{4,5},{5,4},{6,7},{7,6},{8,9},{9,8},{10,11... | collective-permute-start | bytes 3145736 | tf_op jit(solution)/shard_map/ppermute | solution.py:35
  159.9 28.6 %collective-permute-start.27 = (bf16[4,128,1024]{2,1,0:T(8,128)(2,1)S(1)}, bf16[4,128,1024]{2,1,0:T(8,128)(2,1)S(1)}, u32[]{:S(2)}, u32[]{:S(2)}) collective-permute-start(bf16[4,128,1024]{2,1,0:T(8,128)(2,1)S(1)} %shard_map.175.refs_1_), channel_id=1, source_target_pairs={{0,1},{1,0},{2,3},{3,2},{4,5},{5,4},{6,7},{7,6},{8,9},{9,8},{10,11... | collective-permute-start | bytes 3145736 | tf_op jit(solution)/shard_map/ppermute | solution.py:35
  (39 other events, 336.3 us)
